TPU v7x, 256 devices: a whole 4x4x8 slice. The times are simulated.
256 devices in a mesh: sp: 32 (over z, y), tp: 8 (over x, core).
Axes of the slice: x: 4, y: 4, z: 8, core: 2. Of those that a mesh axis runs over, the one named last changes fastest.
Arguments:
- source: bfloat16 [16384, 2048], P(('sp', 'tp')), may hold values from -6 to 6
- target: bfloat16 [4096, 2048], P(('sp', 'tp')), may hold values from -6 to 6
- source_gain: bfloat16 [2, 2048], replicated, may hold values from 0.099609375 to 1.8984375
- target_gain: bfloat16 [2, 2048], replicated, may hold values from 0.099609375 to 1.8984375
- query_weight: bfloat16 [2, 2048, 1024], P(None, None, 'tp'), may hold values from -0.5 to 0.5
- key_weight: bfloat16 [2, 2048, 1024], P(None, None, 'tp'), may hold values from -0.5 to 0.5
- value_weight: bfloat16 [2, 2048, 1024], P(None, None, 'tp'), may hold values from -0.125 to 0.125
- head_gain: bfloat16 [2, 1024], P(None, 'tp'), may hold values from 0.099609375 to 1.8984375
- out_weight: bfloat16 [2, 1024, 2048], P(None, 'tp'), may hold values from -0.1875 to 0.1875
- mlp_gain: bfloat16 [2048], replicated, may hold values from 0.099609375 to 1.8984375
- gate_weight: bfloat16 [2048, 5632], P(None, 'tp'), may hold values from -0.125 to 0.125
- up_weight: bfloat16 [2048, 5632], P(None, 'tp'), may hold values from -0.125 to 0.125
- down_weight: bfloat16 [5632, 2048], P('tp'), may hold values from -0.078125 to 0.078125
Outputs:
- mixed: bfloat16 [4096, 2048], P(('sp', 'tp'))
All inputs are finite; a program needn't handle non-finite values.
Results may differ from a plain program's by a relative error of at most 0.014.
Values may be sent and summed in bfloat16 or wider, within the bound.
A program may use at most 128 MiB of HBM per device.

v0:
```python
import jax
import jax.numpy as jnp
from jax import lax
from jax.sharding import PartitionSpec as P

HEAD_DIM = 128


EPSILON = 1e-06


def in_order(tiles, dim):
    lengths = list(tiles.shape[1:])
    lengths[dim] *= tiles.shape[0]
    return jnp.moveaxis(tiles, 0, dim).reshape(lengths)


def sent_to_all(x, axis):
    devices = lax.axis_size(axis)
    return lax.all_to_all(jnp.broadcast_to(x[None], (devices, *x.shape)), axis, 0, 0, tiled=True)


def collect(x, axis, dim):
    return in_order(sent_to_all(x, axis), dim)


def cut_along(x, dim, devices):
    lengths = x.shape
    tiles = x.reshape(*lengths[:dim], devices, lengths[dim] // devices, *lengths[dim + 1 :])
    return jnp.moveaxis(tiles, dim, 0)


def sent_and_summed(x, axis, dim):
    tiles = cut_along(x, dim, lax.axis_size(axis))
    arrived = lax.all_to_all(tiles, axis, split_axis=0, concat_axis=0, tiled=True)
    return arrived.sum(axis=0)


def row_scale(rows):
    return lax.rsqrt(jnp.mean(rows * rows, axis=-1, keepdims=True) + EPSILON)


def block_stats(queries, key_blocks, value_blocks):
    scores = jnp.einsum(
        "the,bshe->bhts", queries, key_blocks, preferred_element_type=jnp.float32
    ) * HEAD_DIM ** (-0.5)
    block_max = jnp.max(scores, axis=-1)
    weights = jnp.exp(scores - block_max[..., None])
    block_total = jnp.sum(weights, axis=-1)
    block_out = jnp.einsum(
        "bhts,bshe->bthe",
        weights.astype(jnp.bfloat16),
        value_blocks,
        preferred_element_type=jnp.float32,
    ).astype(jnp.bfloat16)
    return (jnp.swapaxes(block_max, 1, 2), jnp.swapaxes(block_total, 1, 2), block_out)


def merge_blocks(carry, stats):
    run_max, run_total, run_out = carry
    block_max, block_total, block_out = stats
    new_max = jnp.max(block_max, axis=0)
    keep = jnp.exp(run_max - new_max)
    factor = jnp.exp(block_max - new_max[None])
    total = run_total * keep + jnp.sum(factor * block_total, axis=0)
    widened = lax.optimization_barrier(block_out).astype(jnp.float32)
    out = run_out * keep[..., None] + jnp.sum(factor[..., None] * widened, axis=0)
    return (new_max, total, out)


def empty_carry(row_count, head_count):
    return (
        jnp.full((row_count, head_count), -jnp.inf, jnp.float32),
        jnp.zeros((row_count, head_count), jnp.float32),
        jnp.zeros((row_count, head_count, HEAD_DIM), jnp.float32),
    )


def local(
    source,
    target,
    source_gain,
    target_gain,
    query_weight,
    key_weight,
    value_weight,
    head_gain,
    out_weight,
    mlp_gain,
    gate_weight,
    up_weight,
    down_weight,
):
    layer_count = query_weight.shape[0]
    width_local = query_weight.shape[2]
    head_count = width_local // HEAD_DIM
    own_rows = target.shape[0]
    group_rows = own_rows * lax.axis_size("tp")
    wide = lax.all_gather(source, "tp", axis=0, tiled=True).astype(jnp.float32)
    scaled = wide * row_scale(wide)
    columns = []
    for project_layer in range(layer_count):
        normed = (scaled * source_gain[project_layer].astype(jnp.float32)).astype(jnp.bfloat16)
        columns.append(
            jnp.dot(normed, key_weight[project_layer], preferred_element_type=jnp.float32).astype(
                jnp.bfloat16
            )
        )
        columns.append(
            jnp.dot(normed, value_weight[project_layer], preferred_element_type=jnp.float32).astype(
                jnp.bfloat16
            )
        )
    projected = jnp.concatenate(columns, axis=1)
    src_rows = projected.shape[0]
    state = target
    for layer in range(layer_count):
        state_wide = state.astype(jnp.float32)
        tgt_normed = (
            state_wide * row_scale(state_wide) * target_gain[layer].astype(jnp.float32)
        ).astype(jnp.bfloat16)

        def project_query(piece, start, layer=layer):
            return jnp.dot(piece, query_weight[layer], preferred_element_type=jnp.float32).astype(
                jnp.bfloat16
            )

        queries = project_query(collect(tgt_normed, "tp", 0), jnp.int32(0))
        queries = queries.reshape(group_rows, head_count, HEAD_DIM)
        offset = 2 * layer * width_local
        keys = projected[:, offset : offset + width_local].reshape(src_rows, head_count, HEAD_DIM)
        values = projected[:, offset + width_local : offset + 2 * width_local].reshape(
            src_rows, head_count, HEAD_DIM
        )
        everyone = collect(queries, "sp", 0)
        block_max, block_total, block_out = block_stats(everyone, keys[None], values[None])
        sp_count = lax.axis_size("sp")
        outgoing = (
            block_out.reshape(sp_count, group_rows, head_count, HEAD_DIM),
            block_max.reshape(sp_count, group_rows, head_count),
            block_total.reshape(sp_count, group_rows, head_count),
        )
        got_out = lax.all_to_all(
            outgoing[0].astype(jnp.float32), "sp", split_axis=0, concat_axis=0, tiled=True
        ).astype(jnp.bfloat16)
        got_max = lax.all_to_all(outgoing[1], "sp", split_axis=0, concat_axis=0, tiled=True)
        got_total = lax.all_to_all(outgoing[2], "sp", split_axis=0, concat_axis=0, tiled=True)
        merged = merge_blocks(
            empty_carry(got_max.shape[1], head_count), (got_max, got_total, got_out)
        )
        attended = merged[2] / merged[1][..., None]
        head_out = (
            attended
            * row_scale(attended)
            * head_gain[layer].astype(jnp.float32).reshape(head_count, HEAD_DIM)
        )
        head_out = head_out.astype(jnp.bfloat16).reshape(group_rows, width_local)

        def mix_heads(start, count, layer=layer, head_out=head_out):
            return jnp.dot(head_out, out_weight[layer], preferred_element_type=jnp.float32)

        mixed_sum = sent_and_summed(
            mix_heads(jnp.int32(0), own_rows * lax.axis_size("tp")), "tp", 0
        )
        state = (state.astype(jnp.float32) + mixed_sum).astype(jnp.bfloat16)
    state_wide = state.astype(jnp.float32)
    mlp_in = (state_wide * row_scale(state_wide) * mlp_gain.astype(jnp.float32)).astype(
        jnp.bfloat16
    )
    piece = lax.all_gather(mlp_in, "tp", axis=0, tiled=True)
    gate = jnp.dot(piece, gate_weight, preferred_element_type=jnp.float32)
    upward = jnp.dot(piece, up_weight, preferred_element_type=jnp.float32)
    hidden = (jax.nn.silu(gate) * upward).astype(jnp.bfloat16)
    down = sent_and_summed(
        jnp.dot(hidden, down_weight, preferred_element_type=jnp.float32), "tp", 0
    )
    return (state_wide + 0.5 * down).astype(jnp.bfloat16)


def solution(mesh):
    in_specs = (
        P(("sp", "tp"), None),
        P(("sp", "tp"), None),
        P(),
        P(),
        P(None, None, "tp"),
        P(None, None, "tp"),
        P(None, None, "tp"),
        P(None, "tp"),
        P(None, "tp", None),
        P(),
        P(None, "tp"),
        P(None, "tp"),
        P("tp", None),
    )
    out_specs = P(("sp", "tp"), None)
    return jax.shard_map(local, mesh=mesh, in_specs=in_specs, out_specs=out_specs, check_vma=False)
```

profile of v0, /device:TPU:1, one launch (start us, length us, event | category | flops | bytes accessed | tf_op | source)
XLA Modules:
  0.0 366.5 jit_solution(14710432905567335046)
XLA Ops:
  10.1 14.9 %all_to_all.65 = bf16[8,16,2048]{2,1,0:T(8,128)(2,1)S(1)} all-to-all(bf16[8,16,2048]{2,1,0:T(8,128)(2,1)S(1)} %broadcast_in_dim.8), channel_id=1, replica_groups=mesh['sp'=32,'tp'=8] {'tp'}, dimensions={0} | all-to-all | bytes 1048576 | tf_op jit(solution)/shard_map/all_to_all | solution.py:20
  27.6 11.3 %all-to-all-start.1 = ((bf16[32,128,1,128]{3,1,2,0:T(8,128)(2,1)}), bf16[32,128,1,128]{3,1,2,0:T(8,128)(2,1)}, u32[]{:S(2)}, u32[]{:S(2)}) async-start(bf16[32,128,1,128]{3,1,2,0:T(8,128)(2,1)} %broadcast_in_dim.9), calls=%async_computation.1 | async-start | bytes 2097152 | tf_op jit(solution)/shard_map/all_to_all | solution.py:20
  43.3 21.6 %all-to-all-done.1 = bf16[32,128,1,128]{3,1,2,0:T(8,128)(2,1)} async-done(((bf16[32,128,1,128]{3,1,2,0:T(8,128)(2,1)}), bf16[32,128,1,128]{3,1,2,0:T(8,128)(2,1)}, u32[]{:S(2)}, u32[]{:S(2)}) %all-to-all-start.1) | async-done | bytes 1048608 | tf_op jit(solution)/shard_map/all_to_all | solution.py:20
  64.9 8.7 %multiply_reduce_fusion.1 = (f32[4096]{0:T(1024)}, f32[512,4096]{1,0:T(8,128)}) fusion(bf16[4096,128]{1,0:T(8,128)(2,1)} %bitcast.5, bf16[512,2048]{1,0:T(8,128)(2,1)} %all-gather.2.cloned.1.call-done, f32[2048]{0:T(1024)S(1)} %bitcast.186, f32[512]{0:T(512)S(1)} %add_rsqrt_fusion, bf16[2,2048,128]{2,1,0:T(8,128)(2,1)} %param.18), kind=kOutput, calls=%fused_computation.5 | convolution fusion | flops 813756416 | bytes 12085248 | tf_op jit(solution)/shard_map/the,bshe->bhts/dot_general | solution.py:44
  73.6 6.4 %all-to-all-start.2 = ((f32[32,128,1]{1,2,0:T(1,128)}), f32[32,128,1]{1,2,0:T(1,128)S(1)}, u32[]{:S(2)}, u32[]{:S(2)}) async-start(f32[32,128,1]{1,2,0:T(1,128)} %bitcast.6), calls=%async_computation.2 | async-start | bytes 32768 | tf_op jit(solution)/shard_map/all_to_all | solution.py:146
  80.0 5.4 %fusion.2 = f32[4096]{0:T(1024)} fusion(f32[512,4096]{1,0:T(8,128)} %get-tuple-element.24, f32[4096]{0:T(1024)} %get-tuple-element.23), kind=kLoop, calls=%fused_computation.6 | loop fusion | flops 6287360 | bytes 8421376 | tf_op jit(solution)/shard_map/reduce_sum | solution.py:49
  88.6 6.1 %all-to-all-start.4 = ((f32[32,128,1]{1,2,0:T(1,128)}), f32[32,128,1]{1,2,0:T(1,128)S(1)}, u32[]{:S(2)}, u32[]{:S(2)}) async-start(f32[32,128,1]{1,2,0:T(1,128)} %bitcast.15), calls=%async_computation.4 | async-start | bytes 32768 | tf_op jit(solution)/shard_map/all_to_all | solution.py:147
  94.6 7.8 %fusion.26 = bf16[16,8,32,128]{3,1,2,0:T(8,128)(2,1)} fusion(f32[512,4096]{1,0:T(8,128)} %get-tuple-element.24, f32[4096]{0:T(1024)} %get-tuple-element.23, bf16[512,2048]{1,0:T(8,128)(2,1)} %all-gather.2.cloned.1.call-done, f32[2048]{0:T(1024)S(1)} %bitcast.187, f32[512]{0:T(512)S(1)} %add_rsqrt_fusion, bf16[2,2048,128]{2,1,0:T(8,128)(2,1)} %param.19), kind=kOutput, calls=%fused_computation.32 | convolution fusion | flops 816381952 | bytes 12085248 | tf_op jit(solution)/shard_map/bhts,bshe->bthe/dot_general | solution.py:50
  105.3 9.5 %all-to-all-start.3 = ((bf16[32,128,1,128]{1,3,2,0:T(8,128)(2,1)}), bf16[32,128,1,128]{1,3,2,0:T(8,128)(2,1)}, u32[]{:S(2)}, u32[]{:S(2)}) async-start(bf16[32,128,1,128]{1,3,2,0:T(8,128)(2,1)} %copy.20), calls=%async_computation.3 | async-start | bytes 2097152 | tf_op jit(solution)/shard_map/all_to_all | solution.py:143
  115.0 24.1 %all-to-all-done.3 = bf16[32,128,1,128]{1,3,2,0:T(8,128)(2,1)} async-done(((bf16[32,128,1,128]{1,3,2,0:T(8,128)(2,1)}), bf16[32,128,1,128]{1,3,2,0:T(8,128)(2,1)}, u32[]{:S(2)}, u32[]{:S(2)}) %all-to-all-start.3) | async-done | bytes 1048608 | tf_op jit(solution)/shard_map/all_to_all | solution.py:143
  142.1 23.0 %all_to_all.66 = f32[8,16,2048]{2,1,0:T(8,128)} all-to-all(f32[8,16,2048]{2,1,0:T(8,128)S(1)} %fusion.48), channel_id=1, replica_groups=mesh['sp'=32,'tp'=8] {'tp'}, dimensions={0} | all-to-all | bytes 2097152 | tf_op jit(solution)/shard_map/all_to_all | solution.py:35
  166.7 12.8 %all_to_all.67 = bf16[8,16,2048]{2,1,0:T(8,128)(2,1)S(1)} all-to-all(bf16[8,16,2048]{2,1,0:T(8,128)(2,1)S(1)} %broadcast_in_dim.10), channel_id=1, replica_groups=mesh['sp'=32,'tp'=8] {'tp'}, dimensions={0} | all-to-all | bytes 1048576 | tf_op jit(solution)/shard_map/all_to_all | solution.py:20
  181.0 31.0 %all_to_all.68 = bf16[32,128,1,128]{3,1,2,0:T(8,128)(2,1)} all-to-all(bf16[32,128,1,128]{3,1,2,0:T(8,128)(2,1)S(1)} %broadcast_in_dim.11), channel_id=1, replica_groups=mesh['sp'=32,'tp'=8] {'sp'}, dimensions={0} | all-to-all | bytes 2097152 | tf_op jit(solution)/shard_map/all_to_all | solution.py:20
  212.0 8.7 %multiply_reduce_fusion = (f32[4096]{0:T(1024)}, f32[512,4096]{1,0:T(8,128)}) fusion(bf16[4096,128]{1,0:T(8,128)(2,1)} %bitcast.176, bf16[512,2048]{1,0:T(8,128)(2,1)} %all-gather.2.cloned.1.call-done, f32[2048]{0:T(1024)S(1)} %bitcast.184, f32[512]{0:T(512)S(1)} %add_rsqrt_fusion, bf16[2,2048,128]{2,1,0:T(8,128)(2,1)} %param.18), kind=kOutput, calls=%fused_computation.4 | convolution fusion | flops 813756416 | bytes 12085248 | tf_op jit(solution)/shard_map/the,bshe->bhts/dot_general | solution.py:44
  220.7 6.4 %all-to-all-start.8 = ((f32[32,128,1]{1,2,0:T(1,128)}), f32[32,128,1]{1,2,0:T(1,128)S(1)}, u32[]{:S(2)}, u32[]{:S(2)}) async-start(f32[32,128,1]{1,2,0:T(1,128)} %bitcast.27), calls=%async_computation.8 | async-start | bytes 32768 | tf_op jit(solution)/shard_map/all_to_all | solution.py:146
  227.1 5.4 %fusion.4 = f32[4096]{0:T(1024)} fusion(f32[512,4096]{1,0:T(8,128)} %get-tuple-element.26, f32[4096]{0:T(1024)} %get-tuple-element.25), kind=kLoop, calls=%fused_computation.8 | loop fusion | flops 6287360 | bytes 8421376 | tf_op jit(solution)/shard_map/reduce_sum | solution.py:49
  235.7 6.0 %all-to-all-start.10 = ((f32[32,128,1]{1,2,0:T(1,128)}), f32[32,128,1]{1,2,0:T(1,128)S(1)}, u32[]{:S(2)}, u32[]{:S(2)}) async-start(f32[32,128,1]{1,2,0:T(1,128)} %bitcast.36), calls=%async_computation.10 | async-start | bytes 32768 | tf_op jit(solution)/shard_map/all_to_all | solution.py:147
  241.7 7.8 %fusion.23 = bf16[16,8,32,128]{3,1,2,0:T(8,128)(2,1)} fusion(f32[512,4096]{1,0:T(8,128)} %get-tuple-element.26, f32[4096]{0:T(1024)} %get-tuple-element.25, bf16[512,2048]{1,0:T(8,128)(2,1)} %all-gather.2.cloned.1.call-done, f32[2048]{0:T(1024)S(1)} %bitcast.185, f32[512]{0:T(512)S(1)} %add_rsqrt_fusion, bf16[2,2048,128]{2,1,0:T(8,128)(2,1)} %param.19), kind=kOutput, calls=%fused_computation.31 | convolution fusion | flops 816381952 | bytes 12085248 | tf_op jit(solution)/shard_map/bhts,bshe->bthe/dot_general | solution.py:50
  252.4 9.3 %all-to-all-start.9 = ((bf16[32,128,1,128]{1,3,2,0:T(8,128)(2,1)}), bf16[32,128,1,128]{1,3,2,0:T(8,128)(2,1)}, u32[]{:S(2)}, u32[]{:S(2)}) async-start(bf16[32,128,1,128]{1,3,2,0:T(8,128)(2,1)} %copy.23), calls=%async_computation.9 | async-start | bytes 2097152 | tf_op jit(solution)/shard_map/all_to_all | solution.py:143
  261.9 24.1 %all-to-all-done.9 = bf16[32,128,1,128]{1,3,2,0:T(8,128)(2,1)} async-done(((bf16[32,128,1,128]{1,3,2,0:T(8,128)(2,1)}), bf16[32,128,1,128]{1,3,2,0:T(8,128)(2,1)}, u32[]{:S(2)}, u32[]{:S(2)}) %all-to-all-start.9) | async-done | bytes 1048608 | tf_op jit(solution)/shard_map/all_to_all | solution.py:143
  290.1 9.0 %all-to-all-start.11 = ((f32[8,16,2048]{2,1,0:T(8,128)}), f32[8,16,2048]{2,1,0:T(8,128)}, u32[]{:S(2)}, u32[]{:S(2)}) async-start(f32[8,16,2048]{2,1,0:T(8,128)} %fusion.41), calls=%async_computation.11 | async-start | bytes 2097152 | tf_op jit(solution)/shard_map/all_to_all | solution.py:35
  299.1 15.1 %all-to-all-done.11 = f32[8,16,2048]{2,1,0:T(8,128)} async-done(((f32[8,16,2048]{2,1,0:T(8,128)}), f32[8,16,2048]{2,1,0:T(8,128)}, u32[]{:S(2)}, u32[]{:S(2)}) %all-to-all-start.11) | async-done | bytes 1048608 | tf_op jit(solution)/shard_map/all_to_all | solution.py:35
  315.8 14.1 %all_gather.7 = bf16[128,2048]{1,0:T(8,128)(2,1)S(1)} all-gather(bf16[16,2048]{1,0:T(8,128)(2,1)S(1)} %fusion.83), channel_id=1, replica_groups=mesh['sp'=32,'tp'=8] {'tp'}, dimensions={0}, use_global_device_ids=true | all-gather | bytes 589824 | tf_op jit(solution)/shard_map/all_gather | solution.py:170
  338.4 19.3 %all_to_all.69 = f32[8,16,2048]{2,1,0:T(8,128)} all-to-all(f32[8,16,2048]{2,1,0:T(8,128)} %bitcast.179), channel_id=1, replica_groups=mesh['sp'=32,'tp'=8] {'tp'}, dimensions={0} | all-to-all | bytes 2097152 | tf_op jit(solution)/shard_map/all_to_all | solution.py:35
  (66 shorter events, 44.9 us)
Async XLA Ops:
  6.5 326.8 %copy-start = (bf16[704,2048]{1,0:T(8,128)(2,1)S(1)}, bf16[704,2048]{1,0:T(8,128)(2,1)}, u32[]{:S(2)}) copy-start(bf16[704,2048]{1,0:T(8,128)(2,1)} %param.25) | copy-start | bytes 8650756
  6.5 32.4 %copy-start.2 = (bf16[2,2048]{1,0:T(2,128)(2,1)S(1)}, bf16[2,2048]{1,0:T(2,128)(2,1)}, u32[]{:S(2)}) copy-start(bf16[2,2048]{1,0:T(2,128)(2,1)} %param.15) | copy-start | bytes 24580
  6.5 34.7 %all-gather.2.cloned.1.call-start = ((), (), s32[]{:S(2)}) async-start(), calls=%async_computation.13 | async-start | bytes 2359296 | tf_op jit(solution)/shard_map/all_gather | solution.py:99
  27.6 37.3 %all-to-all-start.1 = ((bf16[32,128,1,128]{3,1,2,0:T(8,128)(2,1)}), bf16[32,128,1,128]{3,1,2,0:T(8,128)(2,1)}, u32[]{:S(2)}, u32[]{:S(2)}) async-start(bf16[32,128,1,128]{3,1,2,0:T(8,128)(2,1)} %broadcast_in_dim.9), calls=%async_computation.1 | async-start | bytes 2097152 | tf_op jit(solution)/shard_map/all_to_all | solution.py:20
  73.6 14.9 %all-to-all-start.2 = ((f32[32,128,1]{1,2,0:T(1,128)}), f32[32,128,1]{1,2,0:T(1,128)S(1)}, u32[]{:S(2)}, u32[]{:S(2)}) async-start(f32[32,128,1]{1,2,0:T(1,128)} %bitcast.6), calls=%async_computation.2 | async-start | bytes 32768 | tf_op jit(solution)/shard_map/all_to_all | solution.py:146
  88.6 16.7 %all-to-all-start.4 = ((f32[32,128,1]{1,2,0:T(1,128)}), f32[32,128,1]{1,2,0:T(1,128)S(1)}, u32[]{:S(2)}, u32[]{:S(2)}) async-start(f32[32,128,1]{1,2,0:T(1,128)} %bitcast.15), calls=%async_computation.4 | async-start | bytes 32768 | tf_op jit(solution)/shard_map/all_to_all | solution.py:147
  102.5 12.4 %copy-start.4 = (bf16[2,128]{1,0:T(2,128)(2,1)S(1)}, bf16[2,128]{1,0:T(2,128)(2,1)}, u32[]{:S(2)}) copy-start(bf16[2,128]{1,0:T(2,128)(2,1)} %param.20) | copy-start | bytes 1540
  105.3 61.1 %copy-start.1 = (bf16[16,2048]{1,0:T(8,128)(2,1)S(1)}, bf16[16,2048]{1,0:T(8,128)(2,1)}, u32[]{:S(2)}) copy-start(bf16[16,2048]{1,0:T(8,128)(2,1)} %param.14) | copy-start | bytes 196612
  105.3 33.7 %all-to-all-start.3 = ((bf16[32,128,1,128]{1,3,2,0:T(8,128)(2,1)}), bf16[32,128,1,128]{1,3,2,0:T(8,128)(2,1)}, u32[]{:S(2)}, u32[]{:S(2)}) async-start(bf16[32,128,1,128]{1,3,2,0:T(8,128)(2,1)} %copy.20), calls=%async_computation.3 | async-start | bytes 2097152 | tf_op jit(solution)/shard_map/all_to_all | solution.py:143
  220.7 14.9 %all-to-all-start.8 = ((f32[32,128,1]{1,2,0:T(1,128)}), f32[32,128,1]{1,2,0:T(1,128)S(1)}, u32[]{:S(2)}, u32[]{:S(2)}) async-start(f32[32,128,1]{1,2,0:T(1,128)} %bitcast.27), calls=%async_computation.8 | async-start | bytes 32768 | tf_op jit(solution)/shard_map/all_to_all | solution.py:146
  235.7 16.7 %all-to-all-start.10 = ((f32[32,128,1]{1,2,0:T(1,128)}), f32[32,128,1]{1,2,0:T(1,128)S(1)}, u32[]{:S(2)}, u32[]{:S(2)}) async-start(f32[32,128,1]{1,2,0:T(1,128)} %bitcast.36), calls=%async_computation.10 | async-start | bytes 32768 | tf_op jit(solution)/shard_map/all_to_all | solution.py:147
  251.0 48.1 %copy-start.3 = (bf16[2048]{0:T(1024)(128)(2,1)S(1)}, bf16[2048]{0:T(1024)(128)(2,1)}, u32[]{:S(2)}) copy-start(bf16[2048]{0:T(1024)(128)(2,1)} %param.22) | copy-start | bytes 12292
  252.4 33.6 %all-to-all-start.9 = ((bf16[32,128,1,128]{1,3,2,0:T(8,128)(2,1)}), bf16[32,128,1,128]{1,3,2,0:T(8,128)(2,1)}, u32[]{:S(2)}, u32[]{:S(2)}) async-start(bf16[32,128,1,128]{1,3,2,0:T(8,128)(2,1)} %copy.23), calls=%async_computation.9 | async-start | bytes 2097152 | tf_op jit(solution)/shard_map/all_to_all | solution.py:143
  290.1 24.1 %all-to-all-start.11 = ((f32[8,16,2048]{2,1,0:T(8,128)}), f32[8,16,2048]{2,1,0:T(8,128)}, u32[]{:S(2)}, u32[]{:S(2)}) async-start(f32[8,16,2048]{2,1,0:T(8,128)} %fusion.41), calls=%async_computation.11 | async-start | bytes 2097152 | tf_op jit(solution)/shard_map/all_to_all | solution.py:35
Sparse Core Ops, SparseCore 0:
  9.2 31.9 all-gather.1
where the time goes:
time: 368 us; the launch traced here: 366 us
  blocking collectives  115 us (31%)
  waiting for transfers between devices  94.2 us (26%)
  starting transfers between devices  64.1 us (17%)
  matrix products  47.9 us (13%)
  other arithmetic  24.1 us (7%)
  between operations  13.6 us (4%)
  local copies, waits for them, and re-layouts  7.48 us (2%)
    all_to_all x3, blocking collectives, sent_to_all(): lax.all_to_all(jnp.broadcast_to(x[None], (devices, *x.shape)), axis, 0, 0...  58.7 us
    all_to_all x2, waiting for transfers between devices, local(): lax.all_to_all(outgoing[0].astype(jnp.float32), 'sp', split_axis=0, conca...  48.2 us
    all_to_all x2, blocking collectives, sent_and_summed(): lax.all_to_all(tiles, axis, split_axis=0, concat_axis=0, tiled=True)  42.3 us
    all_to_all x1, waiting for transfers between devices, sent_to_all(): lax.all_to_all(jnp.broadcast_to(x[None], (devices, *x.shape)), axis, 0, 0...  21.6 us
    all_to_all x2, starting transfers between devices, local(): lax.all_to_all(outgoing[0].astype(jnp.float32), 'sp', split_axis=0, conca...  18.8 us
    dot_general x2, matrix products, block_stats(): jnp.einsum('the,bshe->bhts', queries, key_blocks, preferred_element_type=...  17.5 us
    dot_general x2, matrix products, block_stats(): jnp.einsum('bhts,bshe->bthe', weights.astype(jnp.bfloat16), value_blocks,...  15.6 us
    all_to_all x1, waiting for transfers between devices, sent_and_summed(): lax.all_to_all(tiles, axis, split_axis=0, concat_axis=0, tiled=True)  15.1 us
  transfers between devices with their start and end apart: 9, of which 7 were waited for; matrix products, arithmetic and copies ran while one was open for 11% of the time, Pallas kernels for 0%

commit v1 on v0

v1 whole, which is shorter than its diff:
```python
import functools
import math

import jax
import jax.numpy as jnp
from jax import lax
from jax.experimental import pallas as pl
from jax.experimental.pallas import tpu as pltpu
from jax.sharding import PartitionSpec as P

HEAD_DIM = 128
EPSILON = 1e-06
NY = 4
MESH = pl.DeviceIdType.MESH
BF16 = jnp.bfloat16
F32 = jnp.float32


def rcopy(src, dst, send, recv, peer):
    return pltpu.make_async_remote_copy(
        src_ref=src,
        dst_ref=dst,
        send_sem=send,
        recv_sem=recv,
        device_id=peer,
        device_id_type=MESH,
    )


def at(index, size):
    return pl.ds(pl.multiple_of(index * size, size), size)


def body(
    nz,
    nx,
    source,
    target,
    source_gain,
    target_gain,
    query_weight,
    key_weight,
    value_weight,
    head_gain,
    out_weight,
    mlp_gain,
    gate_weight,
    up_weight,
    down_weight,
    out,
    src,
    tgt,
    wkv,
    wq,
    sgain,
    tgain,
    mgain,
    hgain,
    wo,
    wg,
    wu,
    wd,
    normed,
    kb,
    vb,
    qb,
    score,
    po,
    ps,
    pr,
    prs,
    ho,
    st,
    hid,
    part,
    pb,
    d2,
    comb,
    fr,
    lsem,
    ag_s,
    ag_r,
    wo_s,
    wo_r,
    k0_s,
    k0_r,
    k1_s,
    k1_r,
    q_s,
    q_r,
    p_s,
    p_r,
    rs_s,
    rs_r,
):
    ntp = 2 * nx
    depth = src.shape[1]
    src_rows = src.shape[0] // ntp
    own_rows = tgt.shape[0] // ntp
    rows = tgt.shape[0]
    block = src.shape[0]
    chunk = 2 * src_rows
    cols = depth // ntp
    hd = HEAD_DIM
    sp = lax.axis_index("sp")
    tp = lax.axis_index("tp")
    z = lax.div(sp, NY)
    y = lax.rem(sp, NY)
    x = lax.div(tp, 2)
    c = lax.rem(tp, 2)

    def device(zz, yy, xx, cc):
        return (zz * NY + yy, xx * 2 + cc)

    def x_peer(d):
        return device(z, y, lax.rem(x + d, nx), c)

    def y_peer(d):
        return device(z, lax.rem(y + d, NY), x, c)

    def z_peer(d):
        return device(lax.rem(z + d, nz), y, x, c)

    partner = device(z, y, x, 1 - c)
    x_order = (1, 3, 2) if nx == 4 else tuple(range(1, nx))

    loads = {}

    def load(name, index, source_ref, to):
        loads[name] = pltpu.make_async_copy(source_ref, to, lsem.at[index])
        loads[name].start()

    load("tgt", 0, target, tgt.at[at(tp, own_rows)])
    load("src", 1, source, src.at[at(tp, src_rows)])
    load("sgain", 2, source_gain, sgain)
    load("k", 3, key_weight, wkv.at[:, :, 0:hd])
    load("v", 4, value_weight, wkv.at[:, :, hd : 2 * hd])
    load("tgain", 5, target_gain, tgain)
    load("q", 6, query_weight, wq)
    load("hgain", 7, head_gain, hgain)
    load("mgain", 8, mlp_gain, mgain)
    load("wo", 9, out_weight.at[:, :, at(tp, cols)], wo.at[:, at(tp, hd)])
    load("wg", 10, gate_weight, wg)
    load("wu", 11, up_weight, wu)
    load("wd", 12, down_weight, wd)

    barrier = pltpu.get_barrier_semaphore()
    peers = [device(z, y, lax.rem(x + d // 2, nx), lax.rem(c + d, 2)) for d in range(1, ntp)]
    peers += [y_peer(d) for d in range(1, NY)]
    peers += [z_peer(d) for d in range(1, nz)]
    for peer in peers:
        pl.semaphore_signal(barrier, inc=1, device_id=peer, device_id_type=MESH)
    pl.semaphore_wait(barrier, len(peers))

    sent = []

    class Gather:
        def __init__(self, index, view):
            self.index = index
            self.view = view
            mine = view(tp)
            s, r = ag_s.at[index], ag_r.at[index]
            self.first = {d: rcopy(mine, mine, s.at[d], r.at[d], x_peer(d)) for d in x_order}
            self.own = rcopy(mine, mine, s.at[0], r.at[0], partner)
            self.passed = {}
            self.own.start()
            for d in x_order:
                self.first[d].start()
            sent.extend([self.own, *self.first.values()])

        def forward(self, d):
            self.first[d].wait_recv()
            owner = lax.rem(x + nx - d, nx) * 2 + c
            s, r = ag_s.at[self.index], ag_r.at[self.index]
            there = self.view(owner)
            self.passed[d] = rcopy(there, there, s.at[nx + d], r.at[nx + d], partner)
            self.passed[d].start()
            sent.append(self.passed[d])

        def finish(self):
            for d in x_order:
                self.forward(d)
            self.own.wait_recv()
            for d in x_order:
                self.passed[d].wait_recv()

    loads["tgt"].wait()
    gather_tgt = Gather(0, lambda j: tgt.at[at(j, own_rows)])
    loads["src"].wait()
    gather_src = Gather(1, lambda j: src.at[at(j, src_rows)])

    for layer in range(2):
        for d in range(1, ntp):
            to = device(z, y, lax.rem(x + d // 2, nx), lax.rem(c + d, 2))
            tp_to = to[1]
            cp = rcopy(
                out_weight.at[layer, :, at(tp_to, cols)],
                wo.at[layer, at(tp, hd)],
                wo_s.at[layer, d],
                wo_r.at[layer, d],
                to,
            )
            cp.start()
            sent.append(cp)

    def wait_wo(layer):
        for d in range(1, ntp):
            rcopy(
                out_weight.at[layer, :, at(tp, cols)],
                wo.at[layer, at(tp, hd)],
                wo_s.at[layer, d],
                wo_r.at[layer, d],
                partner,
            ).wait_recv()

    def norm_rows(from_ref, start, count, gain_ref, gain_row):
        step = 64

        def one(i, carry):
            at_from = pl.ds(pl.multiple_of(start + i * step, step), step)
            at_to = pl.ds(pl.multiple_of(i * step, step), step)
            total = jnp.zeros((step, 128), F32)
            for k in range(0, depth, 128):
                v = from_ref[at_from, k : k + 128].astype(F32)
                total += v * v
            mean = jnp.sum(total, axis=1, keepdims=True) * (1.0 / depth)
            scale = lax.rsqrt(mean + EPSILON)
            for k in range(0, depth, 128):
                v = from_ref[at_from, k : k + 128].astype(F32)
                g = gain_ref[gain_row : gain_row + 1, k : k + 128].astype(F32)
                normed[at_to, k : k + 128] = (v * scale * g).astype(BF16)
            return carry

        lax.fori_loop(0, count // step, one, 0)

    def project_source(layer, xx):
        norm_rows(src, xx * chunk, chunk, sgain, layer)
        kv = jnp.dot(normed[0:chunk], wkv[layer], preferred_element_type=F32)
        first = y * block + xx * chunk
        here = pl.ds(pl.multiple_of(first, chunk), chunk)
        kb[layer, here] = kv[:, 0:hd].astype(BF16)
        vb[layer, :, here] = jnp.transpose(kv[:, hd : 2 * hd]).astype(BF16)

    def k0_copies(xx, d):
        here = pl.ds(pl.multiple_of(y * block + xx * chunk, chunk), chunk)
        k = kb.at[0, here]
        v = vb.at[0, :, here]
        return (
            rcopy(k, k, k0_s.at[0, d, xx], k0_r.at[0, d, xx], y_peer(d)),
            rcopy(v, v, k0_s.at[1, d, xx], k0_r.at[1, d, xx], y_peer(d)),
        )

    def k1_copies(d):
        here = at(y, block)
        k = kb.at[1, here]
        v = vb.at[1, :, here]
        return (
            rcopy(k, k, k1_s.at[0, d], k1_r.at[0, d], y_peer(d)),
            rcopy(v, v, k1_s.at[1, d], k1_r.at[1, d], y_peer(d)),
        )

    def q_copy(layer, d):
        return rcopy(
            qb.at[layer, 0], qb.at[layer, d], q_s.at[layer, d], q_r.at[layer, d], z_peer(d)
        )

    def z_order(i):
        odd = lax.rem(i, 2)
        return odd * lax.div(i + 1, 2) + (1 - odd) * lax.rem(nz - lax.div(i, 2), nz)

    def project_query(layer, state_ref):
        norm_rows(state_ref, 0, rows, tgain, layer)
        q = jnp.dot(normed[0:rows], wq[layer], preferred_element_type=F32)
        qb[layer, 0] = q.astype(BF16)

        def send(i, carry):
            q_copy(layer, z_order(i)).start()
            return carry

        lax.fori_loop(1, nz, send, 0)

    def send_k0(xx):
        for d in (1, 3, 2):
            for cp in k0_copies(xx, d):
                cp.start()

    loads["sgain"].wait()
    loads["k"].wait()
    loads["v"].wait()
    gather_src.own.wait_recv()
    project_source(0, x)
    send_k0(x)
    gather_tgt.finish()
    loads["tgain"].wait()
    loads["q"].wait()
    project_query(0, tgt)
    for d in x_order:
        gather_src.forward(d)
    for d in x_order:
        gather_src.passed[d].wait_recv()
        xx = lax.rem(x + nx - d, nx)
        project_source(0, xx)
        send_k0(xx)

    def project_one(i, carry):
        project_source(1, i)
        return carry

    lax.fori_loop(0, nx, project_one, 0)
    for d in (1, 3, 2):
        for cp in k1_copies(d):
            cp.start()

    factor = math.log2(math.e) * hd**-0.5

    def p_copies(layer, d):
        return (
            rcopy(po.at[layer, d], pr.at[layer, d], p_s.at[layer, 0, d], p_r.at[layer, 0, d], z_peer(nz - d)),
            rcopy(ps.at[layer, d], prs.at[layer, d], p_s.at[layer, 1, d], p_r.at[layer, 1, d], z_peer(nz - d)),
        )

    def attend(layer):
        def one(i, carry):
            d = z_order(i)

            @pl.when(i > 0)
            def _():
                q_copy(layer, d).wait_recv()

            q = qb[layer, d]
            top = None
            for b in range(NY):
                here = slice(b * block, (b + 1) * block)
                s = lax.dot_general(
                    kb[layer, here], q, (((1,), (1,)), ((), ())), preferred_element_type=F32
                )
                score[here] = s
                m = jnp.max(s, axis=0, keepdims=True)
                top = m if top is None else jnp.maximum(top, m)
            shift = top * factor
            total = jnp.zeros((1, rows), F32)
            acc = jnp.zeros((hd, rows), F32)
            for b in range(NY):
                here = slice(b * block, (b + 1) * block)
                w = jnp.exp2(score[here] * factor - shift)
                total += jnp.sum(w, axis=0, keepdims=True)
                acc += jnp.dot(vb[layer, :, here], w.astype(BF16), preferred_element_type=F32)
            low = acc.astype(BF16)
            which = lax.broadcasted_iota(jnp.int32, (8, rows), 0)
            stats = jnp.where(which == 0, top, total)

            @pl.when(i == 0)
            def _():
                pr[layer, 0] = low
                prs[layer, 0] = stats

            @pl.when(i > 0)
            def _():
                po[layer, d] = low
                ps[layer, d] = stats
                for cp in p_copies(layer, d):
                    cp.start()

            return carry

        lax.fori_loop(0, nz, one, 0)

    def merge(layer):
        def wait(d, carry):
            for cp in p_copies(layer, d):
                cp.wait_recv()
            return carry

        lax.fori_loop(1, nz, wait, 0)
        top = prs[layer, 0, 0:1]
        for d in range(1, nz):
            top = jnp.maximum(top, prs[layer, d, 0:1])
        total = jnp.zeros((1, rows), F32)
        acc = jnp.zeros((hd, rows), F32)
        for d in range(nz):
            f = jnp.exp2((prs[layer, d, 0:1] - top) * factor)
            total += f * prs[layer, d, 1:2]
            acc += f * pr[layer, d].astype(F32)
        attended = acc / total
        mean = jnp.mean(attended * attended, axis=0, keepdims=True)
        scaled = jnp.transpose(attended * lax.rsqrt(mean + EPSILON))
        gain = hgain[layer : layer + 1, :].astype(F32)
        ho[layer, :, at(tp, hd)] = (scaled * gain).astype(BF16)

    def advance(layer, old_ref):
        Gather(2 + 2 * layer, lambda j: ho.at[layer, :, at(j, hd)]).finish()
        wait_wo(layer)
        add = jnp.dot(ho[layer], wo[layer], preferred_element_type=F32)
        new = old_ref[:, at(tp, cols)].astype(F32) + add
        st[layer, :, at(tp, cols)] = new.astype(BF16)
        Gather(3 + 2 * layer, lambda j: st.at[layer, :, at(j, cols)]).finish()

    for d in range(1, NY):
        for xx in range(nx):
            for cp in k0_copies(xx, d):
                cp.wait_recv()
    attend(0)
    loads["hgain"].wait()
    loads["wo"].wait()
    merge(0)
    advance(0, tgt)
    project_query(1, st.at[0])
    for d in range(1, NY):
        for cp in k1_copies(d):
            cp.wait_recv()
    attend(1)
    merge(1)
    advance(1, st.at[0])

    loads["mgain"].wait()
    loads["wg"].wait()
    loads["wu"].wait()
    loads["wd"].wait()
    norm_rows(st.at[1], 0, rows, mgain, 0)
    over = (((1,), (1,)), ((), ()))
    gate = lax.dot_general(wg[...], normed[0:rows], over, preferred_element_type=F32)
    up = lax.dot_general(wu[...], normed[0:rows], over, preferred_element_type=F32)
    hid[...] = jnp.transpose(gate / (1.0 + jnp.exp(-gate)) * up).astype(BF16)
    pieces = 2
    width = depth // pieces

    def d2_copy(n):
        w = slice(n * width, (n + 1) * width)
        return rcopy(pb.at[:, :, w], d2.at[:, :, w], rs_s.at[n, 0], rs_r.at[n, 0], partner)

    def fr_copy(n, d):
        w = slice(n * width, (n + 1) * width)
        return rcopy(comb.at[d, :, w], fr.at[d, :, w], rs_s.at[n, d], rs_r.at[n, d], x_peer(d))

    for n in range(pieces):
        w = slice(n * width, (n + 1) * width)
        down = jnp.dot(hid[...], wd[:, w], preferred_element_type=F32)
        part[:, :, :, w] = down.reshape(nx, 2, own_rows, width)
        pb[:, :, w] = part[:, 1 - c, :, w].astype(BF16)
        d2_copy(n).start()
    for n in range(pieces):
        w = slice(n * width, (n + 1) * width)
        d2_copy(n).wait_recv()
        for d in x_order:
            xx = lax.rem(x + d, nx)
            comb[d, :, w] = (part[xx, c, :, w] + d2[xx, :, w].astype(F32)).astype(BF16)
            fr_copy(n, d).start()
    for n in range(pieces):
        w = slice(n * width, (n + 1) * width)
        down = part[x, c, :, w] + d2[x, :, w].astype(F32)
        for d in x_order:
            fr_copy(n, d).wait_recv()
            down += fr[d, :, w].astype(F32)
        state = st[1, at(tp, own_rows), w].astype(F32)
        out[:, w] = (state + 0.5 * down).astype(BF16)

    for cp in sent:
        cp.wait_send()
    for d in range(1, NY):
        for xx in range(nx):
            for cp in k0_copies(xx, d):
                cp.wait_send()
        for cp in k1_copies(d):
            cp.wait_send()
    for layer in range(2):
        for d in range(1, nz):
            q_copy(layer, d).wait_send()
            for cp in p_copies(layer, d):
                cp.wait_send()
    for n in range(pieces):
        d2_copy(n).wait_send()
        for d in x_order:
            fr_copy(n, d).wait_send()


def local(nz, nx, *args):
    source, target = args[0], args[1]
    ntp = 2 * nx
    depth = source.shape[1]
    block = source.shape[0] * ntp
    rows = target.shape[0] * ntp
    own = target.shape[0]
    ffl = args[10].shape[1]
    hd = HEAD_DIM
    args = list(args)
    args[9] = args[9].reshape(1, depth)
    args[10] = args[10].T
    args[11] = args[11].T
    vmem = pltpu.VMEM
    dma = pltpu.SemaphoreType.DMA
    scratch = [
        vmem((block, depth), BF16),
        vmem((rows, depth), BF16),
        vmem((2, depth, 2 * hd), BF16),
        vmem((2, depth, hd), BF16),
        vmem((2, depth), BF16),
        vmem((2, depth), BF16),
        vmem((1, depth), BF16),
        vmem((2, hd), BF16),
        vmem((2, ntp * hd, depth // ntp), BF16),
        vmem((ffl, depth), BF16),
        vmem((ffl, depth), BF16),
        vmem((ffl, depth), BF16),
        vmem((rows, depth), BF16),
        vmem((2, NY * block, hd), BF16),
        vmem((2, hd, NY * block), BF16),
        vmem((2, nz, rows, hd), BF16),
        vmem((NY * block, rows), F32),
        vmem((2, nz, hd, rows), BF16),
        vmem((2, nz, 8, rows), F32),
        vmem((2, nz, hd, rows), BF16),
        vmem((2, nz, 8, rows), F32),
        vmem((2, rows, ntp * hd), BF16),
        vmem((2, rows, depth), BF16),
        vmem((rows, ffl), BF16),
        vmem((nx, 2, own, depth), F32),
        vmem((nx, own, depth), BF16),
        vmem((nx, own, depth), BF16),
        vmem((nx, own, depth), BF16),
        vmem((nx, own, depth), BF16),
        dma((13,)),
        dma((6, 2 * nx)),
        dma((6, 2 * nx)),
        dma((2, ntp)),
        dma((2, ntp)),
        dma((2, NY, nx)),
        dma((2, NY, nx)),
        dma((2, NY)),
        dma((2, NY)),
        dma((2, nz)),
        dma((2, nz)),
        dma((2, 2, nz)),
        dma((2, 2, nz)),
        dma((2, nx)),
        dma((2, nx)),
    ]
    return pl.pallas_call(
        functools.partial(body, nz, nx),
        name="decoder",
        out_shape=jax.ShapeDtypeStruct(target.shape, BF16),
        in_specs=[pl.BlockSpec(memory_space=pl.ANY)] * len(args),
        out_specs=pl.BlockSpec(memory_space=pltpu.VMEM),
        scratch_shapes=scratch,
        compiler_params=pltpu.CompilerParams(
            collective_id=0, has_side_effects=True, vmem_limit_bytes=60 * 1024 * 1024
        ),
    )(*args)


def solution(mesh):
    nz = mesh.shape["sp"] // NY
    nx = mesh.shape["tp"] // 2
    in_specs = (
        P(("sp", "tp"), None),
        P(("sp", "tp"), None),
        P(),
        P(),
        P(None, None, "tp"),
        P(None, None, "tp"),
        P(None, None, "tp"),
        P(None, "tp"),
        P(None, "tp", None),
        P(),
        P(None, "tp"),
        P(None, "tp"),
        P("tp", None),
    )
    out_specs = P(("sp", "tp"), None)
    return jax.shard_map(
        functools.partial(local, nz, nx),
        mesh=mesh,
        in_specs=in_specs,
        out_specs=out_specs,
        check_vma=False,
    )
```

time: 368 us -> 108 us (0.29)
  blocking collectives: 115 us -> 0 us
  Pallas kernels: 0 us -> 105 us
  waiting for transfers between devices: 94.2 us -> 0 us
  starting transfers between devices: 64.1 us -> 0 us
  matrix products: 47.9 us -> 0 us
  other arithmetic: 24.1 us -> 0 us
  between operations: 13.6 us -> 0.01 us
  local copies, waits for them, and re-layouts: 7.48 us -> 2.76 us
    pallas_call x0 -> x1, Pallas kernels: none -> 105 us  [local(): pl.pallas_call(functools.partial(body, nz, nx), name='decoder', out_shape...]
    all_to_all x5 -> x0, blocking collectives: 101 us -> none  [the longest x3 58.7 us: sent_to_all(): lax.all_to_all(jnp.broadcast_to(x[None], (devices, *x.shape)), axis, 0, 0...]
    all_to_all x8 -> x0, waiting for transfers between devices: 91.2 us -> none  [the longest x2 48.2 us: local(): lax.all_to_all(outgoing[0].astype(jnp.float32), 'sp', split_axis=0, conca...]
    all_to_all x8 -> x0, starting transfers between devices: 64.1 us -> none  [the longest x2 18.8 us: local(): lax.all_to_all(outgoing[0].astype(jnp.float32), 'sp', split_axis=0, conca...]
    dot_general x10 -> x0, matrix products: 47.9 us -> none  [the longest x2 17.5 us: block_stats(): jnp.einsum('the,bshe->bhts', queries, key_blocks, preferred_element_type=...]
    reduce_sum x15 -> x0, other arithmetic: 21.1 us -> none  [the longest x2 10.7 us: block_stats(): block_total = jnp.sum(weights, axis=-1)]
    all_gather x1 -> x0, blocking collectives: 14.1 us -> none  [local(): piece = lax.all_gather(mlp_in, 'tp', axis=0, tiled=True)]
  transfers between devices with their start and end apart: 9 -> 0, of which waited for: 7 -> 0; matrix products, arithmetic and copies ran while one was open for 11% -> 0% of each run, Pallas kernels for 0% -> 0%
where the time goes in v1:
time: 108 us
  Pallas kernels  105 us (97%)
  local copies, waits for them, and re-layouts  2.76 us (3%)
    pallas_call x1, Pallas kernels, local(): pl.pallas_call(functools.partial(body, nz, nx), name='decoder', out_shape...  105 us

profile of v1, /device:TPU:1, one launch (start us, length us, event | category | flops | bytes accessed | tf_op | source)
XLA Modules:
  0.0 107.8 jit_solution(11149886550196563856)
XLA Ops:
  0.0 1.3 %reshape.3.mlp_gain = bf16[1,2048]{1,0:T(2,128)(2,1)} reshape(bf16[2048]{0:T(1024)(128)(2,1)} %param.22) | data formatting | bytes 8192 | tf_op jit(solution)/shard_map/reshape | solution.py:486
  1.3 105.0 %decoder.1 = bf16[16,2048]{1,0:T(8,128)(2,1)} custom-call(bf16[64,2048]{1,0:T(8,128)(2,1)} %source.1, bf16[16,2048]{1,0:T(8,128)(2,1)} %target.1, bf16[2,2048]{1,0:T(2,128)(2,1)} %source_gain.1, bf16[2,2048]{1,0:T(2,128)(2,1)} %target_gain.1, bf16[2,2048,128]{2,1,0:T(8,128)(2,1)} %query_weight.1, bf16[2,2048,128]{2,1,0:T(8,128)(2,1)} %key_weight.1, ...), custom_call_target="tpu_custom_call" | custom-call | tf_op jit(solution)/shard_map/decoder/pallas_call | solution.py:537
  106.3 1.5 %copy.15 = bf16[16,2048]{1,0:T(8,128)(2,1)} copy(bf16[16,2048]{1,0:T(8,128)(2,1)} %decoder.1) | data formatting | bytes 131072

commit v2 on v1

v2 whole, which is shorter than its diff:
```python
import functools
import math

import jax
import jax.numpy as jnp
from jax import lax
from jax.experimental import pallas as pl
from jax.experimental.pallas import tpu as pltpu
from jax.sharding import PartitionSpec as P

HEAD_DIM = 128
EPSILON = 1e-06
NY = 4
MESH = pl.DeviceIdType.MESH
BF16 = jnp.bfloat16
F32 = jnp.float32


def rcopy(src, dst, send, recv, peer):
    return pltpu.make_async_remote_copy(
        src_ref=src,
        dst_ref=dst,
        send_sem=send,
        recv_sem=recv,
        device_id=peer,
        device_id_type=MESH,
    )


def at(index, size):
    return pl.ds(pl.multiple_of(index * size, size), size)


def body(
    nz,
    nx,
    source,
    target,
    source_gain,
    target_gain,
    query_weight,
    key_weight,
    value_weight,
    head_gain,
    out_weight,
    mlp_gain,
    gate_weight,
    up_weight,
    down_weight,
    out,
    src,
    tgt,
    wkv,
    wq,
    sgain,
    tgain,
    mgain,
    hgain,
    wo,
    wo1,
    wg,
    wu,
    wd,
    normed,
    kb,
    vb,
    qb,
    score,
    po,
    ps,
    pr,
    prs,
    ho,
    st,
    hid,
    part,
    pb,
    d2,
    comb,
    fr,
    mixed,
    lsem,
    src_s,
    src_r,
    ag_s,
    ag_r,
    wo_s,
    wo_r,
    k_s,
    k_r,
    q_s,
    q0_r,
    q_r,
    p_s,
    p_r,
    d_s,
    d_r,
    f_s,
    f_r,
    o_s,
):
    ntp = 2 * nx
    depth = src.shape[1]
    src_rows = src.shape[0] // ntp
    own_rows = tgt.shape[0] // ntp
    rows = tgt.shape[0]
    block = src.shape[0]
    chunk = 2 * src_rows
    cols = depth // ntp
    hd = HEAD_DIM
    sp = lax.axis_index("sp")
    tp = lax.axis_index("tp")
    z = lax.div(sp, NY)
    y = lax.rem(sp, NY)
    x = lax.div(tp, 2)
    c = lax.rem(tp, 2)

    def device(zz, yy, xx, cc):
        return (zz * NY + yy, xx * 2 + cc)

    def x_peer(d):
        return device(z, y, lax.rem(x + d, nx), c)

    def y_peer(d):
        return device(z, lax.rem(y + d, NY), x, c)

    def z_peer(d):
        return device(lax.rem(z + d, nz), y, x, c)

    partner = device(z, y, x, 1 - c)
    x_order = (1, 3, 2) if nx == 4 else tuple(range(1, nx))

    loads = {}

    def load(name, index, source_ref, to):
        loads[name] = pltpu.make_async_copy(source_ref, to, lsem.at[index])
        loads[name].start()

    load("tgt", 0, target, tgt.at[at(tp, own_rows)])
    load("src", 1, source, src.at[at(tp, src_rows)])
    load("sgain", 2, source_gain, sgain)
    load("k", 3, key_weight, wkv.at[:, :, 0:hd])
    load("v", 4, value_weight, wkv.at[:, :, hd : 2 * hd])
    load("tgain", 5, target_gain, tgain)
    load("q", 6, query_weight, wq)
    load("hgain", 7, head_gain, hgain)
    load("mgain", 8, mlp_gain, mgain)
    load("wo", 9, out_weight.at[0, :, at(tp, cols)], wo.at[at(tp, hd)])
    load("wo1", 13, out_weight.at[1], wo1.at[at(tp, hd)])
    load("wg", 10, gate_weight, wg)
    load("wu", 11, up_weight, wu)
    load("wd", 12, down_weight, wd)

    scope = jax.named_scope
    barrier = pltpu.get_barrier_semaphore()
    peers = [device(z, y, lax.rem(x + d // 2, nx), lax.rem(c + d, 2)) for d in range(1, ntp)]
    peers += [y_peer(d) for d in range(1, NY)]
    peers += [z_peer(d) for d in range(1, nz)]
    with scope("barrier"):
        for peer in peers:
            pl.semaphore_signal(barrier, inc=1, device_id=peer, device_id_type=MESH)
        pl.semaphore_wait(barrier, len(peers))

    def all_sent(ref, sem):
        rcopy(ref, ref, sem, sem, partner).wait_send()

    def all_here(ref, sem):
        rcopy(ref, ref, sem, sem, partner).wait_recv()

    class Gather:
        def __init__(self, index, view):
            self.view = view
            self.send = ag_s.at[index]
            self.near = ag_r.at[index, 0]
            mine = view(tp)
            self.first = {d: rcopy(mine, mine, self.send, ag_r.at[index, d], x_peer(d)) for d in x_order}
            rcopy(mine, mine, self.send, self.near, partner).start()
            for d in x_order:
                self.first[d].start()

        def forward(self):
            for d in x_order:
                self.first[d].wait_recv()
                there = self.view(lax.rem(x + nx - d, nx) * 2 + c)
                rcopy(there, there, self.send, self.near, partner).start()

        def finish(self, near_bytes, sent_bytes):
            all_here(near_bytes, self.near)
            all_sent(sent_bytes, self.send)

    loads["src"].wait()

    half = src_rows // 2
    left, right = x_peer(nx - 1), x_peer(1)
    tp_left = lax.rem(x + nx - 1, nx) * 2 + c
    tp_right = lax.rem(x + 1, nx) * 2 + c
    tp_far = lax.rem(x + 2, nx) * 2 + c

    def src_copy(index, owner, first, count, to):
        ref = src.at[pl.ds(pl.multiple_of(owner * src_rows + first, half), count)]
        rcopy(ref, ref, src_s, src_r.at[index], to).start()

    def src_wait(index, count):
        ref = src.at[pl.ds(0, count)]
        all_here(ref, src_r.at[index])

    src_copy(0, tp, 0, src_rows, partner)
    src_copy(1, tp, 0, half, right)
    src_copy(2, tp, half, half, left)
    src_copy(3, tp, half, half, right)
    src_copy(4, tp, 0, half, left)
    loads["tgt"].wait()
    gather_tgt = Gather(0, lambda j: tgt.at[at(j, own_rows)])

    def out_copy(d):
        to = device(z, y, lax.rem(x + d // 2, nx), lax.rem(c + d, 2))
        return rcopy(
            out_weight.at[0, :, at(to[1], cols)], wo.at[at(tp, hd)], wo_s, wo_r, to
        )

    factor = math.log2(math.e) * hd**-0.5

    def norm_rows(from_ref, start, count, gain_of):
        step = 64

        def one(i, carry):
            at_from = pl.ds(pl.multiple_of(start + i * step, step), step)
            at_to = pl.ds(pl.multiple_of(i * step, step), step)
            total = jnp.zeros((step, 128), F32)
            for k in range(0, depth, 128):
                v = from_ref[at_from, k : k + 128].astype(F32)
                total += v * v
            mean = jnp.sum(total, axis=1, keepdims=True) * (1.0 / depth)
            scale = lax.rsqrt(mean + EPSILON)
            for k in range(0, depth, 128):
                v = from_ref[at_from, k : k + 128].astype(F32)
                g = gain_of(k).astype(F32)
                normed[at_to, k : k + 128] = (v * scale * g).astype(BF16)
            return carry

        lax.fori_loop(0, count // step, one, 0)

    def project_source(layer, xx):
        norm_rows(src, xx * chunk, chunk, lambda k: sgain[layer : layer + 1, k : k + 128])
        kv = jnp.dot(normed[0:chunk], wkv[layer], preferred_element_type=F32)
        first = y * block + xx * chunk
        here = pl.ds(pl.multiple_of(first, chunk), chunk)
        kb[layer, here] = kv[:, 0:hd].astype(BF16)
        vb[layer, :, here] = jnp.transpose(kv[:, hd : 2 * hd]).astype(BF16)

    def k0_copies(xx, d):
        here = pl.ds(pl.multiple_of(y * block + xx * chunk, chunk), chunk)
        k = kb.at[0, here]
        v = vb.at[0, :, here]
        return (
            rcopy(k, k, k_s.at[0, 0], k_r.at[0, 0], y_peer(d)),
            rcopy(v, v, k_s.at[0, 1], k_r.at[0, 1], y_peer(d)),
        )

    def k1_copies(d):
        here = at(y, block)
        k = kb.at[1, here]
        v = vb.at[1, :, here]
        return (
            rcopy(k, k, k_s.at[1, 0], k_r.at[1, 0], y_peer(d)),
            rcopy(v, v, k_s.at[1, 1], k_r.at[1, 1], y_peer(d)),
        )

    def z_order(i):
        odd = lax.rem(i, 2)
        return odd * lax.div(i + 1, 2) + (1 - odd) * lax.rem(nz - lax.div(i, 2), nz)

    def q_copy(layer, slot, source_slot=0, d=None):
        to = z_peer(z_order(slot) if d is None else d)
        return rcopy(
            qb.at[layer, source_slot],
            qb.at[layer, slot],
            q_s.at[layer],
            q0_r if layer == 0 else q_r.at[slot],
            to,
        )

    def project_query(layer, state_ref):
        norm_rows(state_ref, 0, rows, lambda k: tgain[layer : layer + 1, k : k + 128])
        q = jnp.dot(normed[0:rows], wq[layer], preferred_element_type=F32)
        qb[layer, 0] = (q * factor).astype(BF16)

        def send(i, carry):
            q_copy(layer, i).start()
            return carry

        lax.fori_loop(1, nz if layer == 0 else 5, send, 0)

    def send_k0(xx):
        for d in (1, 3, 2):
            for cp in k0_copies(xx, d):
                cp.start()

    with scope("wait_own"):
        loads["sgain"].wait()
        loads["k"].wait()
        loads["v"].wait()
        src_wait(0, src_rows)
    with scope("kv_own"):
        project_source(0, x)
        send_k0(x)
    with scope("wait_src"):
        src_wait(1, half)
        src_copy(5, tp_left, 0, half, right)
        src_wait(2, half)
        src_copy(6, tp_right, half, half, left)
        src_wait(3, half)
        src_copy(7, tp_left, 0, src_rows, partner)
        src_wait(4, half)
        src_copy(8, tp_right, 0, src_rows, partner)
        src_wait(7, src_rows)
    for d in range(1, ntp):
        out_copy(d).start()
    with scope("kv_left"):
        xx = lax.rem(x + nx - 1, nx)
        project_source(0, xx)
        send_k0(xx)
    src_wait(8, src_rows)
    with scope("kv_right"):
        xx = lax.rem(x + 1, nx)
        project_source(0, xx)
        send_k0(xx)
    with scope("wait_tgt"):
        gather_tgt.forward()
        gather_tgt.finish(tgt.at[0 : 4 * own_rows], tgt.at[0 : 7 * own_rows])
        loads["tgain"].wait()
        loads["q"].wait()
    with scope("q0"):
        project_query(0, tgt)
    with scope("wait_far"):
        src_wait(5, half)
        src_copy(9, tp_far, 0, half, partner)
        src_wait(6, half)
        src_copy(10, tp_far, half, half, partner)
        src_wait(9, half)
        src_wait(10, half)
    with scope("kv_far"):
        xx = lax.rem(x + 2, nx)
        project_source(0, xx)
        send_k0(xx)
    loads["wo1"].wait()
    first_rows = 80

    def wo1_first(j):
        return wo1.at[pl.ds(pl.multiple_of(j * hd, hd), first_rows)]

    def wo1_rest(j):
        return wo1.at[pl.ds(pl.multiple_of(j * hd + first_rows, 16), hd - first_rows)]

    gather_wo1 = Gather(3, wo1_first)

    def project_one(i, carry):
        project_source(1, i)
        return carry

    with scope("kv1"):
        lax.fori_loop(0, nx, project_one, 0)
        for d in (1, 3, 2):
            for cp in k1_copies(d):
                cp.start()

    def p_copies(layer, slot):
        to = z_peer(nz - z_order(slot))
        return (
            rcopy(
                po.at[layer, slot], pr.at[layer, slot], p_s.at[layer, 0], p_r.at[layer, 0], to
            ),
            rcopy(
                ps.at[layer, slot], prs.at[layer, slot], p_s.at[layer, 1], p_r.at[layer, 1], to
            ),
        )

    def attend(layer, first, count):
        wide = count * rows
        q = qb[layer, pl.ds(first, count)].reshape(wide, hd)
        top = None
        for b in range(NY):
            here = slice(b * block, (b + 1) * block)
            s = lax.dot_general(
                kb[layer, here], q, (((1,), (1,)), ((), ())), preferred_element_type=F32
            )
            score[here, 0:wide] = s
            m = jnp.max(s, axis=0, keepdims=True)
            top = m if top is None else jnp.maximum(top, m)
        total = jnp.zeros((1, wide), F32)
        acc = jnp.zeros((hd, wide), F32)
        for b in range(NY):
            here = slice(b * block, (b + 1) * block)
            w = jnp.exp2(score[here, 0:wide] - top)
            total += jnp.sum(w, axis=0, keepdims=True)
            acc += jnp.dot(vb[layer, :, here], w.astype(BF16), preferred_element_type=F32)
        low = acc.astype(BF16)
        which = lax.broadcasted_iota(jnp.int32, (8, wide), 0)
        stats = jnp.where(which == 0, top, total)
        for j in range(count):
            to_out, to_stats = (pr, prs) if isinstance(first, int) and first == 0 else (po, ps)
            to_out[layer, first + j] = low[:, j * rows : (j + 1) * rows]
            to_stats[layer, first + j] = stats[:, j * rows : (j + 1) * rows]
            if to_out is po:
                for cp in p_copies(layer, first + j):
                    cp.start()

    def q_wait(layer, slot):
        q_copy(layer, slot).wait_recv()

    def attend_first():
        all_here(qb.at[0, 1:nz], q0_r)
        attend(0, nz - 1, 1)

        def pair(i, carry):
            attend(0, nz - 3 - 2 * i, 2)
            return carry

        lax.fori_loop(0, (nz - 2) // 2, pair, 0)
        attend(0, 0, 1)

    def relays():
        return (
            q_copy(1, 5, 3, 1),
            q_copy(1, 6, 4, nz - 1),
            q_copy(1, 7, 3 + c, 2 + c * (nz - 4)),
        )

    def attend_second():
        attend(1, 0, 1)

        def pair(i, carry):
            first = 1 + 2 * i
            with scope("wait_q"):
                q_wait(1, first)
                q_wait(1, first + 1)

            @pl.when(i == 1)
            def _():
                for cp in relays():
                    cp.start()

            attend(1, first, 2)
            return carry

        lax.fori_loop(0, (nz - 2) // 2, pair, 0)
        with scope("wait_q"):
            q_wait(1, nz - 1)
        attend(1, nz - 1, 1)

    def merge(layer):
        with scope("wait_p"):
            all_here(pr.at[layer, 1:nz], p_r.at[layer, 0])
            all_here(prs.at[layer, 1:nz], p_r.at[layer, 1])
        top = prs[layer, 0, 0:1]
        for d in range(1, nz):
            top = jnp.maximum(top, prs[layer, d, 0:1])
        total = jnp.zeros((1, rows), F32)
        acc = jnp.zeros((hd, rows), F32)
        for d in range(nz):
            f = jnp.exp2(prs[layer, d, 0:1] - top)
            total += f * prs[layer, d, 1:2]
            acc += f * pr[layer, d].astype(F32)
        attended = acc / total
        mean = jnp.mean(attended * attended, axis=0, keepdims=True)
        scaled = jnp.transpose(attended * lax.rsqrt(mean + EPSILON))
        gain = hgain[layer : layer + 1, :].astype(F32)
        ho[layer, :, at(tp, hd)] = (scaled * gain).astype(BF16)

    def gather_heads(layer):
        with scope("gather_ho"):
            gather = Gather(1 if layer == 0 else 5, lambda j: ho.at[layer, :, at(j, hd)])
            gather.forward()
            gather.finish(ho.at[layer, :, 0 : 4 * hd], ho.at[layer, :, 0 : 7 * hd])

    def kv_wait(layer):
        most = (NY - 1) * block
        all_here(kb.at[layer, 0:most], k_r.at[layer, 0])
        all_here(vb.at[layer, :, 0:most], k_r.at[layer, 1])

    with scope("wait_kv0"):
        kv_wait(0)
    with scope("attend0"):
        attend_first()
    loads["hgain"].wait()
    loads["wo"].wait()
    with scope("merge0"):
        merge(0)
    gather_heads(0)
    with scope("wait_wo"):
        all_here(wo.at[0 : (ntp - 1) * hd], wo_r)
    add = jnp.dot(ho[0], wo[...], preferred_element_type=F32)
    new = tgt[:, at(tp, cols)].astype(F32) + add
    st[0, :, at(tp, cols)] = new.astype(BF16)
    with scope("gather_st"):
        gather_st = Gather(2, lambda j: st.at[0, :, at(j, cols)])
        gather_wo1.forward()
        gather_st.forward()
        gather_st.finish(st.at[0, :, 0 : 4 * cols], st.at[0, :, 0 : 7 * cols])
    with scope("wo1"):
        gather_wo1.finish(wo1.at[0 : 4 * first_rows], wo1.at[0 : 7 * first_rows])
        gather_wo1 = Gather(4, wo1_rest)
    with scope("q1"):
        project_query(1, st.at[0])
    with scope("wait_kv1"):
        kv_wait(1)
    with scope("attend1"):
        attend_second()
    with scope("wo1_rest"):
        gather_wo1.forward()
    with scope("merge1"):
        merge(1)
    gather_heads(1)
    with scope("wo1_wait"):
        gather_wo1.finish(
            wo1.at[0 : 4 * (hd - first_rows)], wo1.at[0 : 7 * (hd - first_rows)]
        )
    with scope("out1"):

        def out_piece(i, carry):
            w = at(i, 512)
            add = jnp.dot(ho[1], wo1[:, w], preferred_element_type=F32)
            st[1, :, w] = (st[0, :, w].astype(F32) + add).astype(BF16)
            return carry

        lax.fori_loop(0, depth // 512, out_piece, 0)

    loads["mgain"].wait()
    loads["wg"].wait()
    loads["wu"].wait()
    loads["wd"].wait()
    with scope("mlp_norm"):
        norm_rows(st.at[1], 0, rows, lambda k: mgain[k // 128 : k // 128 + 1, :])
    over = (((1,), (1,)), ((), ()))
    with scope("gate"):
        gate = lax.dot_general(wg[...], normed[0:rows], over, preferred_element_type=F32)
        up = lax.dot_general(wu[...], normed[0:rows], over, preferred_element_type=F32)
        hid[...] = jnp.transpose(gate / (1.0 + jnp.exp(-gate)) * up).astype(BF16)
    pieces = 4
    width = depth // pieces

    def d2_copy(n):
        w = slice(n * width, (n + 1) * width)
        return rcopy(pb.at[:, :, w], d2.at[:, :, w], d_s, d_r.at[n], partner)

    def fr_copy(n, d):
        w = slice(n * width, (n + 1) * width)
        return rcopy(comb.at[d, :, w], fr.at[d, :, w], f_s, f_r.at[n], x_peer(d))

    def pair_sum(n):
        w = slice(n * width, (n + 1) * width)
        with scope("wait_d2"):
            d2_copy(n).wait_recv()
        for d in x_order:
            xx = lax.rem(x + d, nx)
            comb[d, :, w] = (part[xx, c, :, w] + d2[xx, :, w].astype(F32)).astype(BF16)
            fr_copy(n, d).start()

    for n in range(pieces):
        w = slice(n * width, (n + 1) * width)
        with scope("down"):
            down = jnp.dot(hid[...], wd[:, w], preferred_element_type=F32)
            part[:, :, :, w] = down.reshape(nx, 2, own_rows, width)
            pb[:, :, w] = part[:, 1 - c, :, w].astype(BF16)
            d2_copy(n).start()
        if n > 0:
            pair_sum(n - 1)
    pair_sum(pieces - 1)
    def out_piece_copy(n):
        w = slice(n * width, (n + 1) * width)
        return pltpu.make_async_copy(mixed.at[:, w], out.at[:, w], o_s.at[n])

    for n in range(pieces):
        w = slice(n * width, (n + 1) * width)
        down = part[x, c, :, w] + d2[x, :, w].astype(F32)
        with scope("wait_fr"):
            all_here(fr.at[1:nx, :, w], f_r.at[n])
        for d in x_order:
            down += fr[d, :, w].astype(F32)
        state = st[1, at(tp, own_rows), w].astype(F32)
        mixed[:, w] = (state + 0.5 * down).astype(BF16)
        out_piece_copy(n).start()

    with scope("drain"):
        all_sent(src.at[0 : 7 * src_rows], src_s)
        all_sent(wo.at[0 : (ntp - 1) * hd], wo_s)
        for layer in range(2):
            all_sent(kb.at[layer, 0 : (NY - 1) * block], k_s.at[layer, 0])
            all_sent(vb.at[layer, :, 0 : (NY - 1) * block], k_s.at[layer, 1])
            all_sent(qb.at[layer, 1:nz], q_s.at[layer])
            all_sent(po.at[layer, 1:nz], p_s.at[layer, 0])
            all_sent(ps.at[layer, 1:nz], p_s.at[layer, 1])
        all_sent(pb, d_s)
        all_sent(comb.at[1:nx], f_s)
        for n in range(pieces):
            out_piece_copy(n).wait()


def local(nz, nx, *args):
    source, target = args[0], args[1]
    ntp = 2 * nx
    depth = source.shape[1]
    block = source.shape[0] * ntp
    rows = target.shape[0] * ntp
    own = target.shape[0]
    ffl = args[10].shape[1]
    hd = HEAD_DIM
    args = list(args)
    args[9] = args[9].reshape(depth // 128, 128)
    args[10] = args[10].T
    args[11] = args[11].T
    vmem = pltpu.VMEM
    dma = pltpu.SemaphoreType.DMA
    scratch = [
        vmem((block, depth), BF16),
        vmem((rows, depth), BF16),
        vmem((2, depth, 2 * hd), BF16),
        vmem((2, depth, hd), BF16),
        vmem((2, depth), BF16),
        vmem((2, depth), BF16),
        vmem((depth // 128, 128), BF16),
        vmem((2, hd), BF16),
        vmem((ntp * hd, depth // ntp), BF16),
        vmem((ntp * hd, depth), BF16),
        vmem((ffl, depth), BF16),
        vmem((ffl, depth), BF16),
        vmem((ffl, depth), BF16),
        vmem((rows, depth), BF16),
        vmem((2, NY * block, hd), BF16),
        vmem((2, hd, NY * block), BF16),
        vmem((2, nz, rows, hd), BF16),
        vmem((NY * block, 2 * rows), F32),
        vmem((2, nz, hd, rows), BF16),
        vmem((2, nz, 8, rows), F32),
        vmem((2, nz, hd, rows), BF16),
        vmem((2, nz, 8, rows), F32),
        vmem((2, rows, ntp * hd), BF16),
        vmem((2, rows, depth), BF16),
        vmem((rows, ffl), BF16),
        vmem((nx, 2, own, depth), F32),
        vmem((nx, own, depth), BF16),
        vmem((nx, own, depth), BF16),
        vmem((nx, own, depth), BF16),
        vmem((nx, own, depth), BF16),
        vmem((own, depth), BF16),
        dma((14,)),
        dma(()),
        dma((11,)),
        dma((6,)),
        dma((6, nx)),
        dma(()),
        dma(()),
        dma((2, 2)),
        dma((2, 2)),
        dma((2,)),
        dma(()),
        dma((nz,)),
        dma((2, 2)),
        dma((2, 2)),
        dma(()),
        dma((4,)),
        dma(()),
        dma((4,)),
        dma((4,)),
    ]
    return pl.pallas_call(
        functools.partial(body, nz, nx),
        name="decoder",
        out_shape=jax.ShapeDtypeStruct(target.shape, BF16),
        in_specs=[pl.BlockSpec(memory_space=pl.ANY)] * len(args),
        out_specs=pl.BlockSpec(memory_space=pl.ANY),
        scratch_shapes=scratch,
        compiler_params=pltpu.CompilerParams(
            collective_id=0, has_side_effects=True, vmem_limit_bytes=60 * 1024 * 1024
        ),
    )(*args)


def solution(mesh):
    nz = mesh.shape["sp"] // NY
    nx = mesh.shape["tp"] // 2
    in_specs = (
        P(("sp", "tp"), None),
        P(("sp", "tp"), None),
        P(),
        P(),
        P(None, None, "tp"),
        P(None, None, "tp"),
        P(None, None, "tp"),
        P(None, "tp"),
        P(None, "tp", None),
        P(),
        P(None, "tp"),
        P(None, "tp"),
        P("tp", None),
    )
    out_specs = P(("sp", "tp"), None)
    return jax.shard_map(
        functools.partial(local, nz, nx),
        mesh=mesh,
        in_specs=in_specs,
        out_specs=out_specs,
        check_vma=False,
    )
```

time: 108 us -> 90.4 us (0.84)
  Pallas kernels: 105 us -> 88.9 us
  local copies, waits for them, and re-layouts: 2.76 us -> 1.47 us
    pallas_call x1, Pallas kernels: 105 us -> 88.9 us  [local(): pl.pallas_call(functools.partial(body, nz, nx), name='decoder', out_shape...]
    reshape x1 -> x0, local copies, waits for them, and re-layouts: 1.29 us -> none  [local(): args[9] = args[9].reshape(1, depth)]
where the time goes in v2:
time: 90.4 us
  Pallas kernels  88.9 us (98%)
  local copies, waits for them, and re-layouts  1.47 us (2%)
    pallas_call x1, Pallas kernels, local(): pl.pallas_call(functools.partial(body, nz, nx), name='decoder', out_shape...  88.9 us

profile of v2, /device:TPU:1, one launch (start us, length us, event | category | flops | bytes accessed | tf_op | source)
XLA Modules:
  0.0 90.4 jit_solution(12865220573974516724)
XLA Ops:
  0.0 88.9 %decoder.1 = bf16[16,2048]{1,0:T(8,128)(2,1)} custom-call(bf16[64,2048]{1,0:T(8,128)(2,1)} %source.1, bf16[16,2048]{1,0:T(8,128)(2,1)} %target.1, bf16[2,2048]{1,0:T(2,128)(2,1)} %source_gain.1, bf16[2,2048]{1,0:T(2,128)(2,1)} %target_gain.1, bf16[2,2048,128]{2,1,0:T(8,128)(2,1)} %query_weight.1, bf16[2,2048,128]{2,1,0:T(8,128)(2,1)} %key_weight.1, ...), custom_call_target="tpu_custom_call" | custom-call | tf_op jit(solution)/shard_map/decoder/pallas_call | solution.py:666
  88.9 1.5 %copy.15 = bf16[16,2048]{1,0:T(8,128)(2,1)} copy(bf16[16,2048]{1,0:T(8,128)(2,1)} %decoder.1) | data formatting | bytes 131072

commit v3 on v2

--- a/solution.py
+++ b/solution.py
@@ -57,7 +57,6 @@
     mgain,
     hgain,
     wo,
-    wo1,
     wg,
     wu,
     wd,
@@ -84,12 +83,11 @@
     src_r,
     ag_s,
     ag_r,
-    wo_s,
-    wo_r,
+    w_s,
+    w_r,
     k_s,
     k_r,
     q_s,
-    q0_r,
     q_r,
     p_s,
     p_r,
@@ -145,8 +143,8 @@
     load("q", 6, query_weight, wq)
     load("hgain", 7, head_gain, hgain)
     load("mgain", 8, mlp_gain, mgain)
-    load("wo", 9, out_weight.at[0, :, at(tp, cols)], wo.at[at(tp, hd)])
-    load("wo1", 13, out_weight.at[1], wo1.at[at(tp, hd)])
+    load("wo0", 9, out_weight.at[0], wo.at[0, at(tp, hd)])
+    load("wo1", 13, out_weight.at[1], wo.at[1, at(tp, hd)])
     load("wg", 10, gate_weight, wg)
     load("wu", 11, up_weight, wu)
     load("wd", 12, down_weight, wd)
@@ -188,35 +186,65 @@
             all_here(near_bytes, self.near)
             all_sent(sent_bytes, self.send)
 
-    loads["src"].wait()
-
-    half = src_rows // 2
     left, right = x_peer(nx - 1), x_peer(1)
     tp_left = lax.rem(x + nx - 1, nx) * 2 + c
     tp_right = lax.rem(x + 1, nx) * 2 + c
     tp_far = lax.rem(x + 2, nx) * 2 + c
 
-    def src_copy(index, owner, first, count, to):
-        ref = src.at[pl.ds(pl.multiple_of(owner * src_rows + first, half), count)]
-        rcopy(ref, ref, src_s, src_r.at[index], to).start()
-
-    def src_wait(index, count):
-        ref = src.at[pl.ds(0, count)]
-        all_here(ref, src_r.at[index])
-
-    src_copy(0, tp, 0, src_rows, partner)
-    src_copy(1, tp, 0, half, right)
-    src_copy(2, tp, half, half, left)
-    src_copy(3, tp, half, half, right)
-    src_copy(4, tp, 0, half, left)
+    class Spread:
+        def __init__(self, ref, size, send, recv, near):
+            self.ref, self.size, self.half = ref, size, size // 2
+            self.send, self.recv, self.near = send, recv, near
+
+        def copy(self, sem, owner, first, count, to):
+            start = pl.multiple_of(owner * self.size + first, self.half)
+            ref = self.ref.at[pl.ds(start, count)]
+            rcopy(ref, ref, self.send, sem, to).start()
+
+        def wait(self, index):
+            all_here(self.ref.at[pl.ds(0, self.half)], self.recv.at[index])
+
+        def start(self):
+            half = self.half
+            self.copy(self.near[0], tp, 0, self.size, partner)
+            self.copy(self.recv.at[1], tp, 0, half, right)
+            self.copy(self.recv.at[2], tp, half, half, left)
+            self.copy(self.recv.at[3], tp, half, half, right)
+            self.copy(self.recv.at[4], tp, 0, half, left)
+
+        def relay(self):
+            self.wait(1)
+            self.copy(self.recv.at[5], tp_left, 0, self.half, right)
+            self.wait(2)
+            self.copy(self.recv.at[6], tp_right, self.half, self.half, left)
+
+        def forward_sides(self):
+            self.wait(3)
+            self.copy(self.near[1], tp_left, 0, self.size, partner)
+            self.wait(4)
+            self.copy(self.near[2], tp_right, 0, self.size, partner)
+
+        def forward_far(self):
+            self.wait(5)
+            self.copy(self.near[3], tp_far, 0, self.half, partner)
+            self.wait(6)
+            self.copy(self.near[4], tp_far, self.half, self.half, partner)
+
+        def sent(self):
+            all_sent(self.ref.at[0 : 7 * self.size], self.send)
+
+    spread_src = Spread(src, src_rows, src_s, src_r, [src_r.at[i] for i in (0, 7, 8, 9, 10)])
+    spread_wo = [
+        Spread(wo.at[layer], hd, w_s.at[layer], w_r.at[layer], [w_r.at[layer, 0]] * 5)
+        for layer in range(2)
+    ]
+    loads["src"].wait()
+    spread_src.start()
     loads["tgt"].wait()
     gather_tgt = Gather(0, lambda j: tgt.at[at(j, own_rows)])
 
-    def out_copy(d):
-        to = device(z, y, lax.rem(x + d // 2, nx), lax.rem(c + d, 2))
-        return rcopy(
-            out_weight.at[0, :, at(to[1], cols)], wo.at[at(tp, hd)], wo_s, wo_r, to
-        )
+    def src_here(index, count):
+        all_here(src.at[pl.ds(0, count)], src_r.at[index])
 
     factor = math.log2(math.e) * hd**-0.5
 
@@ -276,7 +304,7 @@
             qb.at[layer, source_slot],
             qb.at[layer, slot],
             q_s.at[layer],
-            q0_r if layer == 0 else q_r.at[slot],
+            q_r.at[layer, slot],
             to,
         )
 
@@ -285,11 +313,18 @@
         q = jnp.dot(normed[0:rows], wq[layer], preferred_element_type=F32)
         qb[layer, 0] = (q * factor).astype(BF16)
 
-        def send(i, carry):
-            q_copy(layer, i).start()
-            return carry
-
-        lax.fori_loop(1, nz if layer == 0 else 5, send, 0)
+        for slot in (3, 4, 1, 2):
+            q_copy(layer, slot).start()
+
+    def q_wait(layer, slot):
+        q_copy(layer, slot).wait_recv()
+
+    def relay_queries(layer):
+        q_wait(layer, 3)
+        q_copy(layer, 5, 3, 1).start()
+        q_wait(layer, 4)
+        q_copy(layer, 6, 4, nz - 1).start()
+        q_copy(layer, 7, 3 + c, 2 + c * (nz - 4)).start()
 
     def send_k0(xx):
         for d in (1, 3, 2):
@@ -300,27 +335,19 @@
         loads["sgain"].wait()
         loads["k"].wait()
         loads["v"].wait()
-        src_wait(0, src_rows)
+        src_here(0, src_rows)
     with scope("kv_own"):
         project_source(0, x)
         send_k0(x)
     with scope("wait_src"):
-        src_wait(1, half)
-        src_copy(5, tp_left, 0, half, right)
-        src_wait(2, half)
-        src_copy(6, tp_right, half, half, left)
-        src_wait(3, half)
-        src_copy(7, tp_left, 0, src_rows, partner)
-        src_wait(4, half)
-        src_copy(8, tp_right, 0, src_rows, partner)
-        src_wait(7, src_rows)
-    for d in range(1, ntp):
-        out_copy(d).start()
+        spread_src.relay()
+        spread_src.forward_sides()
+        src_here(7, src_rows)
     with scope("kv_left"):
         xx = lax.rem(x + nx - 1, nx)
         project_source(0, xx)
         send_k0(xx)
-    src_wait(8, src_rows)
+    src_here(8, src_rows)
     with scope("kv_right"):
         xx = lax.rem(x + 1, nx)
         project_source(0, xx)
@@ -332,27 +359,16 @@
         loads["q"].wait()
     with scope("q0"):
         project_query(0, tgt)
+    loads["wo0"].wait()
+    spread_wo[0].start()
     with scope("wait_far"):
-        src_wait(5, half)
-        src_copy(9, tp_far, 0, half, partner)
-        src_wait(6, half)
-        src_copy(10, tp_far, half, half, partner)
-        src_wait(9, half)
-        src_wait(10, half)
+        spread_src.forward_far()
+        src_here(9, src_rows // 2)
+        src_here(10, src_rows // 2)
     with scope("kv_far"):
         xx = lax.rem(x + 2, nx)
         project_source(0, xx)
         send_k0(xx)
-    loads["wo1"].wait()
-    first_rows = 80
-
-    def wo1_first(j):
-        return wo1.at[pl.ds(pl.multiple_of(j * hd, hd), first_rows)]
-
-    def wo1_rest(j):
-        return wo1.at[pl.ds(pl.multiple_of(j * hd + first_rows, 16), hd - first_rows)]
-
-    gather_wo1 = Gather(3, wo1_first)
 
     def project_one(i, carry):
         project_source(1, i)
@@ -360,9 +376,11 @@
 
     with scope("kv1"):
         lax.fori_loop(0, nx, project_one, 0)
-        for d in (1, 3, 2):
-            for cp in k1_copies(d):
-                cp.start()
+    with scope("relay_q0"):
+        relay_queries(0)
+    for d in (1, 3, 2):
+        for cp in k1_copies(d):
+            cp.start()
 
     def p_copies(layer, slot):
         to = z_peer(nz - z_order(slot))
@@ -405,11 +423,9 @@
                 for cp in p_copies(layer, first + j):
                     cp.start()
 
-    def q_wait(layer, slot):
-        q_copy(layer, slot).wait_recv()
-
     def attend_first():
-        all_here(qb.at[0, 1:nz], q0_r)
+        for slot in (1, 2, 5, 6, 7):
+            q_wait(0, slot)
         attend(0, nz - 1, 1)
 
         def pair(i, carry):
@@ -419,34 +435,24 @@
         lax.fori_loop(0, (nz - 2) // 2, pair, 0)
         attend(0, 0, 1)
 
-    def relays():
-        return (
-            q_copy(1, 5, 3, 1),
-            q_copy(1, 6, 4, nz - 1),
-            q_copy(1, 7, 3 + c, 2 + c * (nz - 4)),
-        )
-
     def attend_second():
         attend(1, 0, 1)
-
-        def pair(i, carry):
-            first = 1 + 2 * i
-            with scope("wait_q"):
-                q_wait(1, first)
-                q_wait(1, first + 1)
-
-            @pl.when(i == 1)
-            def _():
-                for cp in relays():
-                    cp.start()
-
-            attend(1, first, 2)
-            return carry
-
-        lax.fori_loop(0, (nz - 2) // 2, pair, 0)
+        with scope("relay_q1"):
+            relay_queries(1)
         with scope("wait_q"):
-            q_wait(1, nz - 1)
-        attend(1, nz - 1, 1)
+            q_wait(1, 1)
+            q_wait(1, 2)
+        attend(1, 1, 2)
+        with scope("relay_wo1"):
+            spread_wo[1].relay()
+        attend(1, 3, 2)
+        with scope("wait_q"):
+            q_wait(1, 5)
+            q_wait(1, 6)
+        attend(1, 5, 2)
+        with scope("wait_q"):
+            q_wait(1, 7)
+        attend(1, 7, 1)
 
     def merge(layer):
         with scope("wait_p"):
@@ -469,9 +475,23 @@
 
     def gather_heads(layer):
         with scope("gather_ho"):
-            gather = Gather(1 if layer == 0 else 5, lambda j: ho.at[layer, :, at(j, hd)])
+            gather = Gather(1 + layer, lambda j: ho.at[layer, :, at(j, hd)])
+            spread_wo[layer].forward_far()
             gather.forward()
             gather.finish(ho.at[layer, :, 0 : 4 * hd], ho.at[layer, :, 0 : 7 * hd])
+
+    def project_heads(layer, old):
+        with scope("wait_wo"):
+            all_here(wo.at[layer, 0 : 4 * hd], w_r.at[layer, 0])
+        with scope("out"):
+
+            def out_piece(i, carry):
+                w = at(i, 512)
+                add = jnp.dot(ho[layer], wo[layer, :, w], preferred_element_type=F32)
+                st[layer, :, w] = (old[:, w].astype(F32) + add).astype(BF16)
+                return carry
+
+            lax.fori_loop(0, depth // 512, out_piece, 0)
 
     def kv_wait(layer):
         most = (NY - 1) * block
@@ -480,50 +500,31 @@
 
     with scope("wait_kv0"):
         kv_wait(0)
+    with scope("relay_wo0"):
+        spread_wo[0].relay()
     with scope("attend0"):
         attend_first()
+    with scope("sides_wo0"):
+        spread_wo[0].forward_sides()
     loads["hgain"].wait()
-    loads["wo"].wait()
     with scope("merge0"):
         merge(0)
     gather_heads(0)
-    with scope("wait_wo"):
-        all_here(wo.at[0 : (ntp - 1) * hd], wo_r)
-    add = jnp.dot(ho[0], wo[...], preferred_element_type=F32)
-    new = tgt[:, at(tp, cols)].astype(F32) + add
-    st[0, :, at(tp, cols)] = new.astype(BF16)
-    with scope("gather_st"):
-        gather_st = Gather(2, lambda j: st.at[0, :, at(j, cols)])
-        gather_wo1.forward()
-        gather_st.forward()
-        gather_st.finish(st.at[0, :, 0 : 4 * cols], st.at[0, :, 0 : 7 * cols])
-    with scope("wo1"):
-        gather_wo1.finish(wo1.at[0 : 4 * first_rows], wo1.at[0 : 7 * first_rows])
-        gather_wo1 = Gather(4, wo1_rest)
+    loads["wo1"].wait()
+    spread_wo[1].start()
+    project_heads(0, tgt)
     with scope("q1"):
         project_query(1, st.at[0])
     with scope("wait_kv1"):
         kv_wait(1)
     with scope("attend1"):
         attend_second()
-    with scope("wo1_rest"):
-        gather_wo1.forward()
+    with scope("sides_wo1"):
+        spread_wo[1].forward_sides()
     with scope("merge1"):
         merge(1)
     gather_heads(1)
-    with scope("wo1_wait"):
-        gather_wo1.finish(
-            wo1.at[0 : 4 * (hd - first_rows)], wo1.at[0 : 7 * (hd - first_rows)]
-        )
-    with scope("out1"):
-
-        def out_piece(i, carry):
-            w = at(i, 512)
-            add = jnp.dot(ho[1], wo1[:, w], preferred_element_type=F32)
-            st[1, :, w] = (st[0, :, w].astype(F32) + add).astype(BF16)
-            return carry
-
-        lax.fori_loop(0, depth // 512, out_piece, 0)
+    project_heads(1, st.at[0])
 
     loads["mgain"].wait()
     loads["wg"].wait()
@@ -568,7 +569,7 @@
     pair_sum(pieces - 1)
     def out_piece_copy(n):
         w = slice(n * width, (n + 1) * width)
-        return pltpu.make_async_copy(mixed.at[:, w], out.at[:, w], o_s.at[n])
+        return pltpu.make_async_copy(mixed.at[:, w], out.at[:, w], o_s)
 
     for n in range(pieces):
         w = slice(n * width, (n + 1) * width)
@@ -582,8 +583,9 @@
         out_piece_copy(n).start()
 
     with scope("drain"):
-        all_sent(src.at[0 : 7 * src_rows], src_s)
-        all_sent(wo.at[0 : (ntp - 1) * hd], wo_s)
+        spread_src.sent()
+        for spread in spread_wo:
+            spread.sent()
         for layer in range(2):
             all_sent(kb.at[layer, 0 : (NY - 1) * block], k_s.at[layer, 0])
             all_sent(vb.at[layer, :, 0 : (NY - 1) * block], k_s.at[layer, 1])
@@ -592,8 +594,7 @@
             all_sent(ps.at[layer, 1:nz], p_s.at[layer, 1])
         all_sent(pb, d_s)
         all_sent(comb.at[1:nx], f_s)
-        for n in range(pieces):
-            out_piece_copy(n).wait()
+        pltpu.make_async_copy(mixed, out, o_s).wait()
 
 
 def local(nz, nx, *args):
@@ -620,8 +621,7 @@
         vmem((2, depth), BF16),
         vmem((depth // 128, 128), BF16),
         vmem((2, hd), BF16),
-        vmem((ntp * hd, depth // ntp), BF16),
-        vmem((ntp * hd, depth), BF16),
+        vmem((2, ntp * hd, depth), BF16),
         vmem((ffl, depth), BF16),
         vmem((ffl, depth), BF16),
         vmem((ffl, depth), BF16),
@@ -646,22 +646,21 @@
         dma((14,)),
         dma(()),
         dma((11,)),
-        dma((6,)),
-        dma((6, nx)),
-        dma(()),
-        dma(()),
+        dma((3,)),
+        dma((3, nx)),
+        dma((2,)),
+        dma((2, 7)),
         dma((2, 2)),
         dma((2, 2)),
         dma((2,)),
-        dma(()),
-        dma((nz,)),
+        dma((2, nz)),
         dma((2, 2)),
         dma((2, 2)),
         dma(()),
         dma((4,)),
         dma(()),
         dma((4,)),
-        dma((4,)),
+        dma(()),
     ]
     return pl.pallas_call(
         functools.partial(body, nz, nx),

time: 90.4 us -> 84.5 us (0.935)
  Pallas kernels: 88.9 us -> 82.9 us
    pallas_call x1, Pallas kernels: 88.9 us -> 82.9 us  [local(): pl.pallas_call(functools.partial(body, nz, nx), name='decoder', out_shape...]
where the time goes in v3:
time: 84.5 us; the launch traced here: 84.4 us
  Pallas kernels  82.9 us (98%)
  local copies, waits for them, and re-layouts  1.47 us (2%)
    pallas_call x1, Pallas kernels, local(): pl.pallas_call(functools.partial(body, nz, nx), name='decoder', out_shape...  82.9 us

profile of v3, /device:TPU:1, one launch (start us, length us, event | category | flops | bytes accessed | tf_op | source)
XLA Modules:
  0.0 84.4 jit_solution(12434025895933558893)
XLA Ops:
  0.0 82.9 %decoder.1 = bf16[16,2048]{1,0:T(8,128)(2,1)} custom-call(bf16[64,2048]{1,0:T(8,128)(2,1)} %source.1, bf16[16,2048]{1,0:T(8,128)(2,1)} %target.1, bf16[2,2048]{1,0:T(2,128)(2,1)} %source_gain.1, bf16[2,2048]{1,0:T(2,128)(2,1)} %target_gain.1, bf16[2,2048,128]{2,1,0:T(8,128)(2,1)} %query_weight.1, bf16[2,2048,128]{2,1,0:T(8,128)(2,1)} %key_weight.1, ...), custom_call_target="tpu_custom_call" | custom-call | tf_op jit(solution)/shard_map/decoder/pallas_call | solution.py:665
  82.9 1.5 %copy.15 = bf16[16,2048]{1,0:T(8,128)(2,1)} copy(bf16[16,2048]{1,0:T(8,128)(2,1)} %decoder.1) | data formatting | bytes 131072

commit v4 on v3

--- a/solution.py
+++ b/solution.py
@@ -87,6 +87,7 @@
     w_r,
     k_s,
     k_r,
+    k0_r,
     q_s,
     q_r,
     p_s,
@@ -240,8 +241,6 @@
     ]
     loads["src"].wait()
     spread_src.start()
-    loads["tgt"].wait()
-    gather_tgt = Gather(0, lambda j: tgt.at[at(j, own_rows)])
 
     def src_here(index, count):
         all_here(src.at[pl.ds(0, count)], src_r.at[index])
@@ -276,14 +275,24 @@
         kb[layer, here] = kv[:, 0:hd].astype(BF16)
         vb[layer, :, here] = jnp.transpose(kv[:, hd : 2 * hd]).astype(BF16)
 
-    def k0_copies(xx, d):
-        here = pl.ds(pl.multiple_of(y * block + xx * chunk, chunk), chunk)
-        k = kb.at[0, here]
-        v = vb.at[0, :, here]
-        return (
-            rcopy(k, k, k_s.at[0, 0], k_r.at[0, 0], y_peer(d)),
-            rcopy(v, v, k_s.at[0, 1], k_r.at[0, 1], y_peer(d)),
-        )
+    def k0_copy(kind, yy, xx, recv, to):
+        here = pl.ds(pl.multiple_of(yy * block + xx * chunk, chunk), chunk)
+        ref = vb.at[0, :, here] if kind else kb.at[0, here]
+        return rcopy(ref, ref, k_s.at[0, kind], recv, to)
+
+    def send_k0(xx):
+        after, before = y_peer(1), y_peer(NY - 1)
+        k0_copy(0, y, xx, k0_r.at[0, xx], after).start()
+        k0_copy(1, y, xx, k0_r.at[1, xx], before).start()
+        k0_copy(0, y, xx, k_r.at[0, 0], before).start()
+        k0_copy(1, y, xx, k_r.at[0, 1], after).start()
+
+    def relay_k0(xx):
+        after, before = y_peer(1), y_peer(NY - 1)
+        k0_copy(0, y, xx, k0_r.at[0, xx], after).wait_recv()
+        k0_copy(0, lax.rem(y + NY - 1, NY), xx, k_r.at[0, 0], after).start()
+        k0_copy(1, y, xx, k0_r.at[1, xx], before).wait_recv()
+        k0_copy(1, lax.rem(y + 1, NY), xx, k_r.at[0, 1], before).start()
 
     def k1_copies(d):
         here = at(y, block)
@@ -325,11 +334,6 @@
         q_wait(layer, 4)
         q_copy(layer, 6, 4, nz - 1).start()
         q_copy(layer, 7, 3 + c, 2 + c * (nz - 4)).start()
-
-    def send_k0(xx):
-        for d in (1, 3, 2):
-            for cp in k0_copies(xx, d):
-                cp.start()
 
     with scope("wait_own"):
         loads["sgain"].wait()
@@ -341,41 +345,51 @@
         send_k0(x)
     with scope("wait_src"):
         spread_src.relay()
+        loads["tgt"].wait()
+        gather_tgt = Gather(0, lambda j: tgt.at[at(j, own_rows)])
         spread_src.forward_sides()
         src_here(7, src_rows)
+    x_left, x_right, x_far = (lax.rem(x + d, nx) for d in (nx - 1, 1, 2))
+    with scope("relay_k0"):
+        relay_k0(x)
     with scope("kv_left"):
-        xx = lax.rem(x + nx - 1, nx)
-        project_source(0, xx)
-        send_k0(xx)
+        project_source(0, x_left)
+        send_k0(x_left)
     src_here(8, src_rows)
     with scope("kv_right"):
-        xx = lax.rem(x + 1, nx)
-        project_source(0, xx)
-        send_k0(xx)
+        project_source(0, x_right)
+        send_k0(x_right)
+    with scope("wait_far"):
+        spread_src.forward_far()
+        src_here(9, src_rows // 2)
+        src_here(10, src_rows // 2)
+    with scope("pass_tgt"):
+        gather_tgt.forward()
+    loads["wo0"].wait()
+    spread_wo[0].start()
+    with scope("kv_far"):
+        project_source(0, x_far)
+        send_k0(x_far)
     with scope("wait_tgt"):
-        gather_tgt.forward()
         gather_tgt.finish(tgt.at[0 : 4 * own_rows], tgt.at[0 : 7 * own_rows])
         loads["tgain"].wait()
         loads["q"].wait()
     with scope("q0"):
         project_query(0, tgt)
-    loads["wo0"].wait()
-    spread_wo[0].start()
-    with scope("wait_far"):
-        spread_src.forward_far()
-        src_here(9, src_rows // 2)
-        src_here(10, src_rows // 2)
-    with scope("kv_far"):
-        xx = lax.rem(x + 2, nx)
-        project_source(0, xx)
-        send_k0(xx)
+    with scope("relay_k0"):
+        relay_k0(x_left)
+        relay_k0(x_right)
 
     def project_one(i, carry):
         project_source(1, i)
         return carry
 
     with scope("kv1"):
-        lax.fori_loop(0, nx, project_one, 0)
+        lax.fori_loop(0, nx // 2, project_one, 0)
+    with scope("relay_k0"):
+        relay_k0(x_far)
+    with scope("kv1"):
+        lax.fori_loop(nx // 2, nx, project_one, 0)
     with scope("relay_q0"):
         relay_queries(0)
     for d in (1, 3, 2):
@@ -424,15 +438,16 @@
                     cp.start()
 
     def attend_first():
-        for slot in (1, 2, 5, 6, 7):
-            q_wait(0, slot)
-        attend(0, nz - 1, 1)
-
-        def pair(i, carry):
-            attend(0, nz - 3 - 2 * i, 2)
-            return carry
-
-        lax.fori_loop(0, (nz - 2) // 2, pair, 0)
+        attend(0, 3, 2)
+        q_wait(0, 1)
+        q_wait(0, 2)
+        attend(0, 1, 2)
+        with scope("wait_q"):
+            q_wait(0, 7)
+        attend(0, 7, 1)
+        q_wait(0, 5)
+        q_wait(0, 6)
+        attend(0, 5, 2)
         attend(0, 0, 1)
 
     def attend_second():
@@ -443,16 +458,16 @@
             q_wait(1, 1)
             q_wait(1, 2)
         attend(1, 1, 2)
+        attend(1, 3, 2)
         with scope("relay_wo1"):
             spread_wo[1].relay()
-        attend(1, 3, 2)
+        with scope("wait_q"):
+            q_wait(1, 7)
+        attend(1, 7, 1)
         with scope("wait_q"):
             q_wait(1, 5)
             q_wait(1, 6)
         attend(1, 5, 2)
-        with scope("wait_q"):
-            q_wait(1, 7)
-        attend(1, 7, 1)
 
     def merge(layer):
         with scope("wait_p"):
@@ -494,7 +509,7 @@
             lax.fori_loop(0, depth // 512, out_piece, 0)
 
     def kv_wait(layer):
-        most = (NY - 1) * block
+        most = (NY - 1 - (layer == 0)) * block
         all_here(kb.at[layer, 0:most], k_r.at[layer, 0])
         all_here(vb.at[layer, :, 0:most], k_r.at[layer, 1])
 
@@ -652,6 +667,7 @@
         dma((2, 7)),
         dma((2, 2)),
         dma((2, 2)),
+        dma((2, nx)),
         dma((2,)),
         dma((2, nz)),
         dma((2, 2)),

time: 84.5 us -> 83.1 us (0.983)
  Pallas kernels: 82.9 us -> 81.5 us
    pallas_call x1, Pallas kernels: 82.9 us -> 81.5 us  [local(): pl.pallas_call(functools.partial(body, nz, nx), name='decoder', out_shape...]
where the time goes in v4:
time: 83.1 us; the launch traced here: 82.9 us
  Pallas kernels  81.5 us (98%)
  local copies, waits for them, and re-layouts  1.47 us (2%)
    pallas_call x1, Pallas kernels, local(): pl.pallas_call(functools.partial(body, nz, nx), name='decoder', out_shape...  81.5 us

profile of v4, /device:TPU:1, one launch (start us, length us, event | category | flops | bytes accessed | tf_op | source)
XLA Modules:
  0.0 82.9 jit_solution(1330125735059046866)
XLA Ops:
  0.0 81.5 %decoder.1 = bf16[16,2048]{1,0:T(8,128)(2,1)} custom-call(bf16[64,2048]{1,0:T(8,128)(2,1)} %source.1, bf16[16,2048]{1,0:T(8,128)(2,1)} %target.1, bf16[2,2048]{1,0:T(2,128)(2,1)} %source_gain.1, bf16[2,2048]{1,0:T(2,128)(2,1)} %target_gain.1, bf16[2,2048,128]{2,1,0:T(8,128)(2,1)} %query_weight.1, bf16[2,2048,128]{2,1,0:T(8,128)(2,1)} %key_weight.1, ...), custom_call_target="tpu_custom_call" | custom-call | tf_op jit(solution)/shard_map/decoder/pallas_call | solution.py:681
  81.5 1.5 %copy.15 = bf16[16,2048]{1,0:T(8,128)(2,1)} copy(bf16[16,2048]{1,0:T(8,128)(2,1)} %decoder.1) | data formatting | bytes 131072

commit v5 on v4

--- a/solution.py
+++ b/solution.py
@@ -127,7 +127,8 @@
         return device(lax.rem(z + d, nz), y, x, c)
 
     partner = device(z, y, x, 1 - c)
-    x_order = (1, 3, 2) if nx == 4 else tuple(range(1, nx))
+    x_order = (1, 3, 2)
+    far_first = (2, 1, 3)
 
     loads = {}
 
@@ -174,7 +175,7 @@
             mine = view(tp)
             self.first = {d: rcopy(mine, mine, self.send, ag_r.at[index, d], x_peer(d)) for d in x_order}
             rcopy(mine, mine, self.send, self.near, partner).start()
-            for d in x_order:
+            for d in far_first:
                 self.first[d].start()
 
         def forward(self):
@@ -490,10 +491,15 @@
 
     def gather_heads(layer):
         with scope("gather_ho"):
-            gather = Gather(1 + layer, lambda j: ho.at[layer, :, at(j, hd)])
+            send, recv = ag_s.at[1 + layer], ag_r.at[1 + layer, 0]
+            mine = ho.at[layer, :, at(tp, hd)]
+            for d in (4, 5, 2, 3, 6, 7, 1):
+                to = device(z, y, lax.rem(x + d // 2, nx), lax.rem(c + d, 2))
+                rcopy(mine, mine, send, recv, to).start()
             spread_wo[layer].forward_far()
-            gather.forward()
-            gather.finish(ho.at[layer, :, 0 : 4 * hd], ho.at[layer, :, 0 : 7 * hd])
+            seven = ho.at[layer, :, 0 : 7 * hd]
+            all_here(seven, recv)
+            all_sent(seven, send)
 
     def project_heads(layer, old):
         with scope("wait_wo"):
@@ -567,7 +573,7 @@
         w = slice(n * width, (n + 1) * width)
         with scope("wait_d2"):
             d2_copy(n).wait_recv()
-        for d in x_order:
+        for d in far_first:
             xx = lax.rem(x + d, nx)
             comb[d, :, w] = (part[xx, c, :, w] + d2[xx, :, w].astype(F32)).astype(BF16)
             fr_copy(n, d).start()
@@ -579,9 +585,8 @@
             part[:, :, :, w] = down.reshape(nx, 2, own_rows, width)
             pb[:, :, w] = part[:, 1 - c, :, w].astype(BF16)
             d2_copy(n).start()
-        if n > 0:
-            pair_sum(n - 1)
-    pair_sum(pieces - 1)
+    for n in range(pieces):
+        pair_sum(n)
     def out_piece_copy(n):
         w = slice(n * width, (n + 1) * width)
         return pltpu.make_async_copy(mixed.at[:, w], out.at[:, w], o_s)

time: 83.1 us -> 81.3 us (0.978)
  Pallas kernels: 81.5 us -> 79.7 us
    pallas_call x1, Pallas kernels: 81.5 us -> 79.7 us  [local(): pl.pallas_call(functools.partial(body, nz, nx), name='decoder', out_shape...]
where the time goes in v5:
time: 81.3 us; the launch traced here: 81.2 us
  Pallas kernels  79.7 us (98%)
  local copies, waits for them, and re-layouts  1.47 us (2%)
    pallas_call x1, Pallas kernels, local(): pl.pallas_call(functools.partial(body, nz, nx), name='decoder', out_shape...  79.7 us

profile of v5, /device:TPU:1, one launch (start us, length us, event | category | flops | bytes accessed | tf_op | source)
XLA Modules:
  0.0 81.2 jit_solution(15590499906175856032)
XLA Ops:
  0.0 79.7 %decoder.1 = bf16[16,2048]{1,0:T(8,128)(2,1)} custom-call(bf16[64,2048]{1,0:T(8,128)(2,1)} %source.1, bf16[16,2048]{1,0:T(8,128)(2,1)} %target.1, bf16[2,2048]{1,0:T(2,128)(2,1)} %source_gain.1, bf16[2,2048]{1,0:T(2,128)(2,1)} %target_gain.1, bf16[2,2048,128]{2,1,0:T(8,128)(2,1)} %query_weight.1, bf16[2,2048,128]{2,1,0:T(8,128)(2,1)} %key_weight.1, ...), custom_call_target="tpu_custom_call" | custom-call | tf_op jit(solution)/shard_map/decoder/pallas_call | solution.py:686
  79.7 1.5 %copy.15 = bf16[16,2048]{1,0:T(8,128)(2,1)} copy(bf16[16,2048]{1,0:T(8,128)(2,1)} %decoder.1) | data formatting | bytes 131072

commit v6 on v5

--- a/solution.py
+++ b/solution.py
@@ -217,14 +217,16 @@
         def relay(self):
             self.wait(1)
             self.copy(self.recv.at[5], tp_left, 0, self.half, right)
+            self.copy(self.near[1], tp_left, 0, self.half, partner)
             self.wait(2)
             self.copy(self.recv.at[6], tp_right, self.half, self.half, left)
+            self.copy(self.near[2], tp_right, self.half, self.half, partner)
 
         def forward_sides(self):
             self.wait(3)
-            self.copy(self.near[1], tp_left, 0, self.size, partner)
+            self.copy(self.near[1], tp_left, self.half, self.half, partner)
             self.wait(4)
-            self.copy(self.near[2], tp_right, 0, self.size, partner)
+            self.copy(self.near[2], tp_right, 0, self.half, partner)
 
         def forward_far(self):
             self.wait(5)
@@ -266,7 +268,7 @@
                 normed[at_to, k : k + 128] = (v * scale * g).astype(BF16)
             return carry
 
-        lax.fori_loop(0, count // step, one, 0)
+        lax.fori_loop(0, count // step, one, 0, unroll=True)
 
     def project_source(layer, xx):
         norm_rows(src, xx * chunk, chunk, lambda k: sgain[layer : layer + 1, k : k + 128])
@@ -440,16 +442,16 @@
 
     def attend_first():
         attend(0, 3, 2)
-        q_wait(0, 1)
-        q_wait(0, 2)
-        attend(0, 1, 2)
+        attend(0, 0, 1)
         with scope("wait_q"):
             q_wait(0, 7)
         attend(0, 7, 1)
         q_wait(0, 5)
         q_wait(0, 6)
         attend(0, 5, 2)
-        attend(0, 0, 1)
+        q_wait(0, 1)
+        q_wait(0, 2)
+        attend(0, 1, 2)
 
     def attend_second():
         attend(1, 0, 1)
@@ -507,12 +509,12 @@
         with scope("out"):
 
             def out_piece(i, carry):
-                w = at(i, 512)
+                w = at(i, 1024)
                 add = jnp.dot(ho[layer], wo[layer, :, w], preferred_element_type=F32)
                 st[layer, :, w] = (old[:, w].astype(F32) + add).astype(BF16)
                 return carry
 
-            lax.fori_loop(0, depth // 512, out_piece, 0)
+            lax.fori_loop(0, depth // 1024, out_piece, 0)
 
     def kv_wait(layer):
         most = (NY - 1 - (layer == 0)) * block

time: 81.3 us -> 80.6 us (level)
  no operation moved by 1% of the time
where the time goes in v6:
time: 80.6 us; the launch traced here: 80.5 us
  Pallas kernels  79 us (98%)
  local copies, waits for them, and re-layouts  1.47 us (2%)
    pallas_call x1, Pallas kernels, local(): pl.pallas_call(functools.partial(body, nz, nx), name='decoder', out_shape...  79 us

profile of v6, /device:TPU:1, one launch (start us, length us, event | category | flops | bytes accessed | tf_op | source)
XLA Modules:
  0.0 80.5 jit_solution(1249342003122766814)
XLA Ops:
  0.0 79.0 %decoder.1 = bf16[16,2048]{1,0:T(8,128)(2,1)} custom-call(bf16[64,2048]{1,0:T(8,128)(2,1)} %source.1, bf16[16,2048]{1,0:T(8,128)(2,1)} %target.1, bf16[2,2048]{1,0:T(2,128)(2,1)} %source_gain.1, bf16[2,2048]{1,0:T(2,128)(2,1)} %target_gain.1, bf16[2,2048,128]{2,1,0:T(8,128)(2,1)} %query_weight.1, bf16[2,2048,128]{2,1,0:T(8,128)(2,1)} %key_weight.1, ...), custom_call_target="tpu_custom_call" | custom-call | tf_op jit(solution)/shard_map/decoder/pallas_call | solution.py:688
  79.0 1.5 %copy.15 = bf16[16,2048]{1,0:T(8,128)(2,1)} copy(bf16[16,2048]{1,0:T(8,128)(2,1)} %decoder.1) | data formatting | bytes 131072
